TPU v7x, 32 devices: a whole 2x2x4 slice. The times are simulated.
32 devices in a mesh: sp: 8 (over z, y), tp: 4 (over x, core).
Axes of the slice: x: 2, y: 2, z: 4, core: 2. Of those that a mesh axis runs over, the one named last changes fastest.
Arguments:
- inputs: bfloat16 [2048, 4096], P('sp', 'tp'), may hold values from -6 to 6
- input_norm_gain: bfloat16 [4096], replicated, may hold values from 0.099609375 to 1.8984375
- pooling_input_weight: bfloat16 [4096, 2048], P('sp', 'tp'), may hold values from -0.09375 to 0.09375
- query_weight: bfloat16 [4096, 2048], P('sp', 'tp'), may hold values from -0.09375 to 0.09375
- key_weight: bfloat16 [4096, 2048], P('sp', 'tp'), may hold values from -0.09375 to 0.09375
- value_weight: bfloat16 [4096, 2048], P('sp', 'tp'), may hold values from -0.09375 to 0.09375
- gate_weight: bfloat16 [4096, 2048], P('sp', 'tp'), may hold values from -0.09375 to 0.09375
- decay_weight: bfloat16 [4096, 16], replicated, may hold values from -0.25 to 0.25
- strength_weight: bfloat16 [4096, 16], replicated, may hold values from -0.09375 to 0.09375
- pooling_group_map: bfloat16 [16, 128, 128], P('tp'), may hold values from -0.5 to 0.5
- pooling_scale: float32 [2048], P('tp'), may hold values from 0.1 to 1.9
- head_log_decay: float32 [16], P('tp')
- decay_logit_bias: float32 [16], P('tp'), may hold values from -1 to 1
- write_logit_bias: float32 [16], P('tp')
- decay_position_factor: float32 [2048, 16], P('sp', 'tp'), may hold values from 0.28 to 3.25
- decay_position_offset: float32 [2048, 16], P('sp', 'tp'), may hold values from -0.7 to 0
- head_norm_gain: float32 [128], replicated, may hold values from 0.1 to 1.9
- pooling_output_weight: bfloat16 [2048, 4096], P('tp', 'sp'), may hold values from -0.125 to 0.125
- delta_output_weight: bfloat16 [2048, 4096], P('tp', 'sp'), may hold values from -0.125 to 0.125
Outputs:
- mixed_out: bfloat16 [2048, 4096], P('sp', 'tp')
All inputs are finite; a program needn't handle non-finite values.
Results may differ from a plain program's by a relative error of at most 0.02.
Values may be sent and summed in bfloat16 or wider, within the bound.
A program may use at most 128 MiB of HBM per device.

v0:
```python
import jax
import jax.numpy as jnp
from jax import lax
from jax.sharding import PartitionSpec as P

HD = 128
PC = 128
BLK = 64


epsilon = 1e-06
highest = lax.Precision.HIGHEST


def shifted(value, axis, steps):
    count = lax.axis_size(axis)
    leading, last = (max(0, -steps), min(count, count - steps))
    return lax.ppermute(value, axis, [(source, source + steps) for source in range(leading, last)])


def unit_rows(matrix):
    return matrix * lax.rsqrt(jnp.sum(matrix * matrix, axis=-1, keepdims=True) + epsilon)


def pool_windows(first_group, group_count):
    group_ids = first_group + jnp.arange(group_count, dtype=jnp.int32)
    return 2 ** (1 + group_ids % 4)


def pool_branch(padded, windows, positions, pooling_group_map, pooling_scale):
    row_count = padded.shape[0] - 16
    window_sum = jnp.zeros(padded[16:].shape, jnp.float32)
    for lag_index in range(16):
        window_part = padded[16 - lag_index : 16 - lag_index + row_count]
        window_sum = (
            window_sum + window_part * (lag_index < windows).astype(jnp.float32)[None, :, None]
        )
    counts = jnp.minimum(positions[:, None] + 1, windows[None, :]).astype(jnp.float32)
    mixed = window_sum / counts[..., None] - padded[16:]
    projected = jnp.einsum(
        "tgc,gcd->tgd", mixed, pooling_group_map.astype(jnp.float32), precision=highest
    )
    return (projected.reshape(row_count, -1) * pooling_scale).astype(jnp.bfloat16)


def delta_rule_inputs(
    query_row_block,
    key_matrix_rows,
    value_row_block,
    decay_logits,
    write_logits,
    head_log_decay,
    decay_logit_bias,
    write_logit_bias,
    decay_position_factor,
    decay_position_offset,
):
    row_count = query_row_block.shape[0]
    head_count = head_log_decay.shape[0]

    def heads_of(matrix):
        return jax.nn.silu(matrix.astype(jnp.float32)).reshape(row_count, head_count, HD)

    query_matrix = unit_rows(heads_of(query_row_block)) * HD ** (-0.5)
    incoming_keys = unit_rows(heads_of(key_matrix_rows))
    value_matrix = heads_of(value_row_block)
    write_strength_rows = jax.nn.sigmoid(write_logits + write_logit_bias)
    decay_log_rows = (
        -jnp.exp(head_log_decay)
        * jax.nn.softplus(decay_logits + decay_logit_bias)
        * decay_position_factor
        + decay_position_offset
    )
    return (query_matrix, incoming_keys, value_matrix, write_strength_rows, decay_log_rows)


def block_terms(query_matrix, incoming_keys, value_matrix, write_strength_rows, decay_log_rows):
    length, head_count, head_depth = query_matrix.shape
    blocks = length // BLK

    def regroup(member):
        return member.reshape(blocks, BLK, head_count, -1).transpose(2, 0, 1, 3)

    query_matrix, incoming_keys, value_matrix = (
        regroup(query_matrix),
        regroup(incoming_keys),
        regroup(value_matrix),
    )
    write_strength_rows = write_strength_rows.reshape(blocks, BLK, head_count).transpose(2, 0, 1)
    running = jnp.cumsum(
        decay_log_rows.reshape(blocks, BLK, head_count).transpose(2, 0, 1), axis=-1
    )
    positions = jnp.arange(BLK)
    causal = positions[:, None] >= positions[None, :]
    strict = positions[:, None] > positions[None, :]
    spread = running[..., :, None] - running[..., None, :]
    decay_table = jnp.where(causal, jnp.exp(jnp.where(causal, spread, 0.0)), 0.0)
    weighted = incoming_keys * write_strength_rows[..., None]
    lower_part = jnp.where(
        strict,
        jnp.einsum("hnid,hnjd->hnij", weighted, incoming_keys, precision=highest) * decay_table,
        0.0,
    )
    system = lower_part + jnp.eye(BLK, dtype=jnp.float32)
    corrected = jax.scipy.linalg.solve_triangular(
        system, value_matrix * write_strength_rows[..., None], lower=True
    )
    erased = jax.scipy.linalg.solve_triangular(
        system, weighted * jnp.exp(running)[..., None], lower=True
    )
    scores = (
        jnp.einsum("hnid,hnjd->hnij", query_matrix, incoming_keys, precision=highest) * decay_table
    )
    query_decayed = query_matrix * jnp.exp(running)[..., None]
    block_total = running[..., -1]
    key_decayed = incoming_keys * jnp.exp(block_total[..., None] - running)[..., None]
    return (corrected, erased, query_decayed, key_decayed, scores, block_total)


def run_blocks(state_start, terms):

    def advance(state_now, pieces):
        corrected, erased, query_decayed, key_decayed, scores, block_total = pieces
        fresh_values = corrected - jnp.einsum("hcd,hde->hce", erased, state_now, precision=highest)
        output = jnp.einsum("hcd,hde->hce", query_decayed, state_now, precision=highest)
        output = output + jnp.einsum("hij,hje->hie", scores, fresh_values, precision=highest)
        state_now = state_now * jnp.exp(block_total)[:, None, None]
        state_now = state_now + jnp.einsum(
            "hcd,hce->hde", key_decayed, fresh_values, precision=highest
        )
        return (state_now, output)

    stacked = tuple((jnp.moveaxis(member, 1, 0) for member in terms))
    final_state, outputs = lax.scan(advance, state_start, stacked)
    blocks, head_count, block_rows, head_depth = outputs.shape
    return (
        final_state,
        outputs.transpose(0, 2, 1, 3).reshape(blocks * block_rows, head_count, head_depth),
    )


def compose_maps(terms):
    corrected, erased, query_decayed, key_decayed, scores, block_total = terms
    head_count, blocks, block_rows, head_depth = corrected.shape
    start_map = jnp.concatenate(
        [
            jnp.broadcast_to(
                jnp.eye(head_depth, dtype=jnp.float32), (head_count, head_depth, head_depth)
            ),
            jnp.zeros((head_count, head_depth, head_depth), jnp.float32),
        ],
        axis=-1,
    )

    def absorb(joined_map, pieces):
        corrected_block, erased_block, key_block, total_block = pieces
        target = jnp.concatenate([jnp.zeros_like(corrected_block), corrected_block], axis=-1)
        residue = target - jnp.einsum("hcd,hde->hce", erased_block, joined_map, precision=highest)
        updated = joined_map * jnp.exp(total_block)[:, None, None]
        updated = updated + jnp.einsum("hcd,hce->hde", key_block, residue, precision=highest)
        return (updated, None)

    stacked = tuple(
        (jnp.moveaxis(member, 1, 0) for member in (corrected, erased, key_decayed, block_total))
    )
    joined_map, unused = lax.scan(absorb, start_map, stacked)
    return (joined_map[..., :head_depth], joined_map[..., head_depth:])


def delta_finish(outputs, gate_rows, head_norm_gain):
    row_count, head_count, head_depth = outputs.shape
    scaled = (
        outputs
        * lax.rsqrt(jnp.mean(outputs * outputs, axis=-1, keepdims=True) + epsilon)
        * head_norm_gain
    )
    gated = scaled * jax.nn.silu(
        gate_rows.astype(jnp.float32).reshape(row_count, head_count, head_depth)
    )
    return gated.reshape(row_count, head_count * head_depth).astype(jnp.bfloat16)


def per_device(
    inputs,
    input_norm_gain,
    pooling_input_weight,
    query_weight,
    key_weight,
    value_weight,
    gate_weight,
    decay_weight,
    strength_weight,
    pooling_group_map,
    pooling_scale,
    head_log_decay,
    decay_logit_bias,
    write_logit_bias,
    decay_position_factor,
    decay_position_offset,
    head_norm_gain,
    pooling_output_weight,
    delta_output_weight,
):
    tok_rows = inputs.shape[0]
    gathered = lax.all_gather(inputs, "tp", axis=1, tiled=True)
    floats = gathered.astype(jnp.float32)
    normed = (
        floats
        * lax.rsqrt(jnp.mean(floats * floats, axis=-1, keepdims=True) + epsilon)
        * input_norm_gain.astype(jnp.float32)
    ).astype(jnp.bfloat16)
    head_count = head_log_decay.shape[0]
    head_first = lax.axis_index("tp") * head_count
    rate_weights = jnp.concatenate(
        [
            lax.dynamic_slice_in_dim(decay_weight, head_first, head_count, 1),
            lax.dynamic_slice_in_dim(strength_weight, head_first, head_count, 1),
        ],
        axis=1,
    )
    rate_rows = jnp.dot(normed, rate_weights, preferred_element_type=jnp.float32)
    decay_logits = rate_rows[:, :head_count]
    write_logits = rate_rows[:, head_count:]
    weights = (pooling_input_weight, query_weight, key_weight, value_weight, gate_weight)
    widths = [member.shape[1] for member in weights]
    joined = jnp.concatenate(weights, axis=1)
    feature_columns = lax.all_to_all(normed, "sp", split_axis=1, concat_axis=0, tiled=True)
    summed_rows = lax.psum_scatter(
        jnp.dot(feature_columns, joined, preferred_element_type=jnp.float32).astype(jnp.bfloat16),
        "sp",
        scatter_dimension=0,
        tiled=True,
    ).astype(jnp.float32)
    split_points = [sum(widths[: split_index + 1]) for split_index in range(len(widths) - 1)]
    projected = jnp.split(summed_rows, split_points, axis=1)
    pool_rows, query_row_block, key_matrix_rows, value_row_block, gate_rows = (
        member.astype(jnp.bfloat16) for member in projected
    )
    previous = shifted(pool_rows[tok_rows - 16 :], "sp", 1)
    group_count = pooling_group_map.shape[0]
    padded = (
        jnp.concatenate([previous, pool_rows], axis=0)
        .astype(jnp.float32)
        .reshape(tok_rows + 16, group_count, PC)
    )
    positions = lax.axis_index("sp") * tok_rows + jnp.arange(tok_rows, dtype=jnp.int32)
    pool_out = pool_branch(
        padded,
        pool_windows(lax.axis_index("tp") * group_count, group_count),
        positions,
        pooling_group_map,
        pooling_scale,
    )
    query_matrix, incoming_keys, value_matrix, write_strength_rows, decay_log_rows = (
        delta_rule_inputs(
            query_row_block,
            key_matrix_rows,
            value_row_block,
            decay_logits,
            write_logits,
            head_log_decay,
            decay_logit_bias,
            write_logit_bias,
            decay_position_factor,
            decay_position_offset,
        )
    )
    terms = block_terms(
        query_matrix, incoming_keys, value_matrix, write_strength_rows, decay_log_rows
    )
    transition = compose_maps(terms)
    identity = (
        jnp.broadcast_to(jnp.eye(HD, dtype=jnp.float32), (head_count, HD, HD)),
        jnp.zeros((head_count, HD, HD), jnp.float32),
    )

    def pass_state(step_index, state_now):
        advanced = (
            jnp.einsum("hij,hjk->hik", transition[0], state_now, precision=highest) + transition[1]
        )
        return shifted(advanced.astype(jnp.bfloat16), "sp", 1).astype(advanced.dtype)

    state_in = lax.fori_loop(0, lax.axis_size("sp") - 1, pass_state, identity[1])
    unused_state, outputs = run_blocks(state_in, terms)
    delta_out = delta_finish(outputs, gate_rows, head_norm_gain)
    both_out = jnp.concatenate([pool_out, delta_out], axis=1)
    out_weights = jnp.concatenate([pooling_output_weight, delta_output_weight], axis=0)
    partial_value = jnp.dot(
        both_out,
        lax.all_gather(out_weights, "sp", axis=1, tiled=True),
        preferred_element_type=jnp.float32,
    )
    summed = lax.psum_scatter(
        partial_value.astype(jnp.bfloat16), "tp", scatter_dimension=1, tiled=True
    )
    return summed


def solution(mesh):
    placed = (
        P("sp", "tp"),
        P(),
        P("sp", "tp"),
        P("sp", "tp"),
        P("sp", "tp"),
        P("sp", "tp"),
        P("sp", "tp"),
        P(),
        P(),
        P("tp", None, None),
        P("tp"),
        P("tp"),
        P("tp"),
        P("tp"),
        P("sp", "tp"),
        P("sp", "tp"),
        P(),
        P("tp", "sp"),
        P("tp", "sp"),
    )
    return jax.shard_map(
        per_device, mesh=mesh, in_specs=placed, out_specs=P("sp", "tp"), check_vma=False
    )
```

profile of v0, /device:TPU:0, one launch (start us, length us, event | category | flops | bytes accessed | tf_op | source)
XLA Modules:
  0.0 527.2 jit_solution(4660057743608130236)
XLA Ops:
  6.5 2.1 copy.256
  9.3 24.9 %all-gather.3.cloned.1.call-done = bf16[256,4096]{0,1:T(8,128)(2,1)} async-done(((bf16[256,1024]{0,1:T(8,128)(2,1)}), bf16[256,4096]{0,1:T(8,128)(2,1)}) %all-gather.3.cloned.1.call-update) | async-done | bytes 2097168 | tf_op jit(solution)/shard_map/all_gather | solution.py:205
  34.2 2.3 fusion.30
  36.5 1.7 fusion.32
  38.3 5.6 %all-to-all-start = ((bf16[256,8,512]{0,2,1:T(8,128)(2,1)}), bf16[256,8,512]{0,2,1:T(8,128)(2,1)S(1)}, u32[]{:S(2)}, u32[]{:S(2)}) async-start(bf16[256,8,512]{0,2,1:T(8,128)(2,1)} %bitcast.11), calls=%async_computation | async-start | bytes 4194304 | tf_op jit(solution)/shard_map/all_to_all | solution.py:227
  44.0 0.9 constant_dynamic-update-slice_fusion.4
  44.8 0.9 constant_dynamic-update-slice_fusion.3
  45.7 1.9 constant_dynamic-update-slice_fusion.2
  47.6 0.9 constant_dynamic-update-slice_fusion.1
  48.5 0.9 constant_dynamic-update-slice_fusion
  49.4 43.2 %all-to-all-done = bf16[256,8,512]{0,2,1:T(8,128)(2,1)S(1)} async-done(((bf16[256,8,512]{0,2,1:T(8,128)(2,1)}), bf16[256,8,512]{0,2,1:T(8,128)(2,1)S(1)}, u32[]{:S(2)}, u32[]{:S(2)}) %all-to-all-start) | async-done | bytes 2097184 | tf_op jit(solution)/shard_map/all_to_all | solution.py:227
  92.5 2.4 copy.257
  94.9 10.3 %convolution_convert_fusion = bf16[2048,2560]{1,0:T(8,128)(2,1)} fusion(bf16[2048,512]{1,0:T(8,128)(2,1)} %bitcast.301, bf16[512,2560]{1,0:T(8,128)(2,1)} %constant_dynamic-update-slice_fusion), kind=kOutput, calls=%fused_computation.39 | convolution fusion | flops 5373952000 | bytes 15204352 | tf_op jit(solution)/shard_map/dot_general | solution.py:229
  105.3 0.9 copy-done.9
  106.4 1.1 pad_maximum_fusion
  114.8 0.9 constant_dynamic-slice_fusion.2
  115.8 2.0 fusion.135
  118.0 0.9 reduce_window_sum.13
  122.9 158.8 %reduce-scatter.3.cloned.1.call-done = bf16[256,2560]{1,0:T(8,128)(2,1)} async-done(((bf16[2048,2560]{1,0:T(8,128)(2,1)}), bf16[256,2560]{1,0:T(8,128)(2,1)}) %reduce-scatter.3.cloned.1.call-update) | async-done | bytes 1310736 | tf_op jit(solution)/shard_map/reduce_scatter | solution.py:228
  281.7 1.3 slice.158
  283.0 4.0 collective-permute-start.1
  287.0 2.4 fusion.154
  290.9 1.3 reshape_reshape.3
  293.0 2.2 broadcast_multiply_fusion
  295.2 1.7 fusion.36
  296.9 78.8 %custom-call.5 = f32[4,4,1,64,64]{3,4,2,1,0:T(8,128)S(1)} custom-call(f32[4,4,1,64,64]{4,3,2,1,0:T(8,128)S(1)} %fusion.36), custom_call_target="InvertDiagBlocksLowerTriangular" | custom-call | tf_op jit(solution)/shard_map/jit(_solve_triangular)/vmap(vmap())/triangular_solve | solution.py:105
  375.8 2.1 convolution_bitcast_fusion.1
  378.0 1.0 convolution_bitcast_fusion.2
  379.4 7.6 %while.33 = (s32[]{:T(128)}, f32[4,128,256]{2,1,0:T(8,128)S(1)}, f32[4,4]{1,0:T(4,128)}, f32[4,4,64,128]{3,2,1,0:T(8,128)S(1)}, f32[4,4,64,128]{3,2,1,0:T(8,128)S(1)}, /*index=5*/f32[4,4,64,128]{3,2,1,0:T(8,128)S(1)}, s32[]{:T(128)}) while((s32[]{:T(128)}, f32[4,128,256]{2,1,0:T(8,128)S(1)}, f32[4,4]{1,0:T(4,128)}, ...), condition=%wide.region_5.7_spmd, body=%wide.region_4.6_spmd.sunk | while | flops 201654272 | bytes 2753149 | solution.py:166
  382.5 0.8 convolution_add_fusion.6
  384.4 0.7 convolution_add_fusion.6
  386.3 0.7 convolution_add_fusion.6
  387.1 1.8 bitcast_multiply_fusion.18
  388.9 2.9 fusion.37
  391.8 58.0 %while.35 = (s32[]{:T(128)}, f32[4,128,128]{2,1,0:T(8,128)S(1)}, f32[4,128,128]{2,1,0:T(8,128)S(1)}, f32[4,128,128]{2,1,0:T(8,128)S(1)}, s32[]{:T(128)}, /*index=5*/s32[]{:T(128)}) while((s32[]{:T(128)}, f32[4,128,128]{2,1,0:T(8,128)S(1)}, f32[4,128,128]{2,1,0:T(8,128)S(1)}, f32[4,128,128]{2,1,0:T(8,128)S(1)}, s32[]{:T(128)}, ...), condition=%wide.region_7.9_spmd.clone, body=%wide.region_6.8_spmd.clone.sunk | while | flops 100925440 | bytes 1835127 | solution.py:283
  392.2 1.4 collective-permute-start
  393.6 2.6 collective-permute-done
  396.6 6.9 %collective-permute-start = (bf16[4,128,128]{2,1,0:T(8,128)(2,1)S(1)}, bf16[4,128,128]{2,1,0:T(8,128)(2,1)S(1)}, u32[]{:S(2)}, u32[]{:S(2)}) collective-permute-start(bf16[4,128,128]{2,1,0:T(8,128)(2,1)S(1)} %fusion.207), channel_id=1, source_target_pairs={{0,4},{4,8},{8,12},{12,16},{16,20},{20,24},{24,28},{1,5},{5,9},{9,... | collective-permute-start | bytes 393224 | tf_op jit(solution)/shard_map/while/body/eval_jaxpr/ppermute | solution.py:18
  403.5 2.5 collective-permute-done
  406.4 7.8 %collective-permute-start = (bf16[4,128,128]{2,1,0:T(8,128)(2,1)S(1)}, bf16[4,128,128]{2,1,0:T(8,128)(2,1)S(1)}, u32[]{:S(2)}, u32[]{:S(2)}) collective-permute-start(bf16[4,128,128]{2,1,0:T(8,128)(2,1)S(1)} %fusion.207), channel_id=1, source_target_pairs={{0,4},{4,8},{8,12},{12,16},{16,20},{20,24},{24,28},{1,5},{5,9},{9,... | collective-permute-start | bytes 393224 | tf_op jit(solution)/shard_map/while/body/eval_jaxpr/ppermute | solution.py:18
  414.2 2.5 collective-permute-done
  417.2 5.3 %collective-permute-start = (bf16[4,128,128]{2,1,0:T(8,128)(2,1)S(1)}, bf16[4,128,128]{2,1,0:T(8,128)(2,1)S(1)}, u32[]{:S(2)}, u32[]{:S(2)}) collective-permute-start(bf16[4,128,128]{2,1,0:T(8,128)(2,1)S(1)} %fusion.207), channel_id=1, source_target_pairs={{0,4},{4,8},{8,12},{12,16},{16,20},{20,24},{24,28},{1,5},{5,9},{9,... | collective-permute-start | bytes 393224 | tf_op jit(solution)/shard_map/while/body/eval_jaxpr/ppermute | solution.py:18
  422.5 2.5 collective-permute-done
  425.4 5.3 collective-permute-start
  430.7 2.5 collective-permute-done
  433.6 5.3 collective-permute-start
  438.9 2.5 collective-permute-done
  441.8 5.4 %collective-permute-start = (bf16[4,128,128]{2,1,0:T(8,128)(2,1)S(1)}, bf16[4,128,128]{2,1,0:T(8,128)(2,1)S(1)}, u32[]{:S(2)}, u32[]{:S(2)}) collective-permute-start(bf16[4,128,128]{2,1,0:T(8,128)(2,1)S(1)} %fusion.207), channel_id=1, source_target_pairs={{0,4},{4,8},{8,12},{12,16},{16,20},{20,24},{24,28},{1,5},{5,9},{9,... | collective-permute-start | bytes 393224 | tf_op jit(solution)/shard_map/while/body/eval_jaxpr/ppermute | solution.py:18
  447.2 2.5 collective-permute-done
  449.8 16.6 %while.34 = (s32[]{:T(128)}, f32[4,128,128]{2,1,0:T(8,128)S(1)}, f32[4,4,64,128]{3,2,1,0:T(8,128)S(1)}, f32[4,4]{1,0:T(4,128)}, f32[4,4,64,128]{3,2,1,0:T(8,128)...) while((s32[]{:T(128)}, f32[4,128,128]{2,1,0:T(8,128)S(1)}, ...), condition=%wide.region_10.12_spmd, body=%wide.region_9.11_spmd.sunk | while | flops 176357376 | bytes 2493581 | solution.py:134
  450.2 1.2 fusion.203
  451.3 1.3 fusion.204
  454.3 1.2 fusion.203
  455.5 1.3 fusion.204
  458.5 1.2 fusion.203
  459.6 1.3 fusion.204
  462.6 1.2 fusion.203
  463.8 1.3 fusion.204
  467.5 1.1 fusion.113
  468.6 0.8 maximum_convert_fusion
  469.6 1.0 slice_bitcast_fusion.15
  470.8 1.8 fusion.55
  472.8 7.1 %convolution_convert_fusion.1 = bf16[256,4096]{1,0:T(8,128)(2,1)} fusion(bf16[1024,4096]{1,0:T(8,128)(2,1)} %all-gather.5.cloned.1.call-done, bf16[256,512]{1,0:T(8,128)(2,1)S(1)} %fusion.113, bf16[256,512]{1,0:T(8,128)(2,1)S(1)} %multiply_convert_fusion), kind=kOutput, calls=%fused_computation.42 | convolution fusion | flops 2149580800 | bytes 11010048 | tf_op jit(solution)/shard_map/dot_general | solution.py:288
  479.9 40.7 %reduce-scatter.5.cloned.1.call-done = bf16[256,1024]{1,0:T(8,128)(2,1)} async-done(((bf16[256,4096]{1,0:T(8,128)(2,1)}), bf16[256,1024]{1,0:T(8,128)(2,1)}) %reduce-scatter.5.cloned.1.call-update) | async-done | bytes 524304 | tf_op jit(solution)/shard_map/reduce_scatter | solution.py:293
  (185 shorter events, 31.5 us)
Async XLA Ops:
  6.5 464.0 %copy-start = (bf16[4,128,128]{2,1,0:T(8,128)(2,1)S(1)}, bf16[4,128,128]{2,1,0:T(8,128)(2,1)}, u32[]{:S(2)}) copy-start(bf16[4,128,128]{2,1,0:T(8,128)(2,1)} %param.36) | copy-start | bytes 393220
  6.5 27.7 %all-gather.3.cloned.1.call-start = ((), (), s32[]{:S(2)}) async-start(), calls=%async_computation.3 | async-start | bytes 2621440 | tf_op jit(solution)/shard_map/all_gather | solution.py:205
  34.2 2.3 copy-start.1
  38.3 5.7 %copy-start.5 = (bf16[512,512]{1,0:T(8,128)(2,1)S(1)}, bf16[512,512]{1,0:T(8,128)(2,1)}, u32[]{:S(2)}) copy-start(bf16[512,512]{1,0:T(8,128)(2,1)} %param.29) | copy-start | bytes 1572868
  38.3 6.6 %copy-start.6 = (bf16[512,512]{1,0:T(8,128)(2,1)S(1)}, bf16[512,512]{1,0:T(8,128)(2,1)}, u32[]{:S(2)}) copy-start(bf16[512,512]{1,0:T(8,128)(2,1)} %param.30) | copy-start | bytes 1572868
  38.3 54.3 %all-to-all-start = ((bf16[256,8,512]{0,2,1:T(8,128)(2,1)}), bf16[256,8,512]{0,2,1:T(8,128)(2,1)S(1)}, u32[]{:S(2)}, u32[]{:S(2)}) async-start(bf16[256,8,512]{0,2,1:T(8,128)(2,1)} %bitcast.11), calls=%async_computation | async-start | bytes 4194304 | tf_op jit(solution)/shard_map/all_to_all | solution.py:227
  43.9 237.8 %reduce-scatter.3.cloned.1.call-start = ((), (), s32[]{:S(2)}) async-start(), calls=%async_computation.4 | async-start | bytes 11796480 | tf_op jit(solution)/shard_map/reduce_scatter | solution.py:228
  44.0 3.6 copy-start.7
  44.0 4.6 copy-start.8
  105.2 1.0 copy-start.9
  105.2 1.2 copy-start.10
  105.2 8.3 %copy-start.36 = (f32[128]{0:T(128)S(1)}, f32[128]{0:T(128)}, u32[]{:S(2)}) copy-start(f32[128]{0:T(128)} %param.43) | copy-start | bytes 1540
  105.2 10.5 %copy-start.39 = (f32[4]{0:T(128)S(1)}, f32[4]{0:T(128)}, u32[]{:S(2)}) copy-start(f32[4]{0:T(128)} %param.38) | copy-start | bytes 52
  105.2 367.6 %all-gather.5.cloned.1.call-start = ((), (), s32[]{:S(2)}) async-start(), calls=%async_computation.5 | async-start | bytes 9437184 | tf_op jit(solution)/shard_map/all_gather | solution.py:290
  107.5 10.3 %copy-start.17 = (f32[256,4]{0,1:T(4,128)S(1)}, f32[256,4]{0,1:T(4,128)}, u32[]{:S(2)}) copy-start(f32[256,4]{0,1:T(4,128)} %param.42) | copy-start | bytes 12292
  107.5 10.3 %copy-start.18 = (f32[256,4]{0,1:T(4,128)S(1)}, f32[256,4]{0,1:T(4,128)}, u32[]{:S(2)}) copy-start(f32[256,4]{0,1:T(4,128)} %param.41) | copy-start | bytes 12292
  107.5 10.3 %copy-start.37 = (f32[4]{0:T(128)S(1)}, f32[4]{0:T(128)}, u32[]{:S(2)}) copy-start(f32[4]{0:T(128)} %param.40) | copy-start | bytes 52
  107.5 10.3 %copy-start.38 = (f32[4]{0:T(128)S(1)}, f32[4]{0:T(128)}, u32[]{:S(2)}) copy-start(f32[4]{0:T(128)} %param.39) | copy-start | bytes 52
  107.5 413.2 %reduce-scatter.5.cloned.1.call-start = ((), (), s32[]{:S(2)}) async-start(), calls=%async_computation.6 | async-start | bytes 2621440 | tf_op jit(solution)/shard_map/reduce_scatter | solution.py:293
  283.0 185.6 %collective-permute-start.1 = (bf16[16,512]{1,0:T(8,128)(2,1)}, bf16[16,512]{1,0:T(8,128)(2,1)}, u32[]{:S(2)}, u32[]{:S(2)}) collective-permute-start(bf16[16,512]{1,0:T(8,128)(2,1)} %slice.158), channel_id=1, source_target_pairs={{0,4},{4,8},{8,12},{12,16},{16,20},{20,24},{24,28},{1,5},{5,9},{9,... | collective-permute-start | bytes 49160 | tf_op jit(solution)/shard_map/ppermute | solution.py:18
  293.0 2.2 copy-start.14
  295.2 80.6 %copy-start.3 = (f32[4,4,64,128]{3,2,0,1:T(8,128)}, f32[4,4,64,128]{3,2,0,1:T(8,128)S(1)}, u32[]{:S(2)}) copy-start(f32[4,4,64,128]{3,2,0,1:T(8,128)S(1)} %get-tuple-element.255) | copy-start | bytes 1572868
  375.8 2.2 copy-start.4
  375.8 3.2 copy-start.11
  375.8 3.2 copy-start.13
  379.4 9.5 %copy-start.12 = (f32[4,4,64]{2,1,0:T(4,128)S(1)}, f32[4,4,64]{2,1,0:T(4,128)}, u32[]{:S(2)}) copy-start(f32[4,4,64]{2,1,0:T(4,128)} %copy.298) | copy-start | bytes 12292
  391.8 58.0 %copy-start.2 = (f32[4,4,64,128]{3,2,1,0:T(8,128)S(1)}, f32[4,4,64,128]{3,2,1,0:T(8,128)}, u32[]{:S(2)}) copy-start(f32[4,4,64,128]{3,2,1,0:T(8,128)} %custom-call.8) | copy-start | bytes 1572868
  392.2 4.0 collective-permute-start
  396.6 9.4 %collective-permute-start = (bf16[4,128,128]{2,1,0:T(8,128)(2,1)S(1)}, bf16[4,128,128]{2,1,0:T(8,128)(2,1)S(1)}, u32[]{:S(2)}, u32[]{:S(2)}) collective-permute-start(bf16[4,128,128]{2,1,0:T(8,128)(2,1)S(1)} %fusion.207), channel_id=1, source_target_pairs={{0,4},{4,8},{8,12},{12,16},{16,20},{20,24},{24,28},{1,5},{5,9},{9,... | collective-permute-start | bytes 393224 | tf_op jit(solution)/shard_map/while/body/eval_jaxpr/ppermute | solution.py:18
  406.4 10.3 %collective-permute-start = (bf16[4,128,128]{2,1,0:T(8,128)(2,1)S(1)}, bf16[4,128,128]{2,1,0:T(8,128)(2,1)S(1)}, u32[]{:S(2)}, u32[]{:S(2)}) collective-permute-start(bf16[4,128,128]{2,1,0:T(8,128)(2,1)S(1)} %fusion.207), channel_id=1, source_target_pairs={{0,4},{4,8},{8,12},{12,16},{16,20},{20,24},{24,28},{1,5},{5,9},{9,... | collective-permute-start | bytes 393224 | tf_op jit(solution)/shard_map/while/body/eval_jaxpr/ppermute | solution.py:18
  417.2 7.8 %collective-permute-start = (bf16[4,128,128]{2,1,0:T(8,128)(2,1)S(1)}, bf16[4,128,128]{2,1,0:T(8,128)(2,1)S(1)}, u32[]{:S(2)}, u32[]{:S(2)}) collective-permute-start(bf16[4,128,128]{2,1,0:T(8,128)(2,1)S(1)} %fusion.207), channel_id=1, source_target_pairs={{0,4},{4,8},{8,12},{12,16},{16,20},{20,24},{24,28},{1,5},{5,9},{9,... | collective-permute-start | bytes 393224 | tf_op jit(solution)/shard_map/while/body/eval_jaxpr/ppermute | solution.py:18
  425.4 7.8 %collective-permute-start = (bf16[4,128,128]{2,1,0:T(8,128)(2,1)S(1)}, bf16[4,128,128]{2,1,0:T(8,128)(2,1)S(1)}, u32[]{:S(2)}, u32[]{:S(2)}) collective-permute-start(bf16[4,128,128]{2,1,0:T(8,128)(2,1)S(1)} %fusion.207), channel_id=1, source_target_pairs={{0,4},{4,8},{8,12},{12,16},{16,20},{20,24},{24,28},{1,5},{5,9},{9,... | collective-permute-start | bytes 393224 | tf_op jit(solution)/shard_map/while/body/eval_jaxpr/ppermute | solution.py:18
  433.6 7.8 %collective-permute-start = (bf16[4,128,128]{2,1,0:T(8,128)(2,1)S(1)}, bf16[4,128,128]{2,1,0:T(8,128)(2,1)S(1)}, u32[]{:S(2)}, u32[]{:S(2)}) collective-permute-start(bf16[4,128,128]{2,1,0:T(8,128)(2,1)S(1)} %fusion.207), channel_id=1, source_target_pairs={{0,4},{4,8},{8,12},{12,16},{16,20},{20,24},{24,28},{1,5},{5,9},{9,... | collective-permute-start | bytes 393224 | tf_op jit(solution)/shard_map/while/body/eval_jaxpr/ppermute | solution.py:18
  441.8 7.9 %collective-permute-start = (bf16[4,128,128]{2,1,0:T(8,128)(2,1)S(1)}, bf16[4,128,128]{2,1,0:T(8,128)(2,1)S(1)}, u32[]{:S(2)}, u32[]{:S(2)}) collective-permute-start(bf16[4,128,128]{2,1,0:T(8,128)(2,1)S(1)} %fusion.207), channel_id=1, source_target_pairs={{0,4},{4,8},{8,12},{12,16},{16,20},{20,24},{24,28},{1,5},{5,9},{9,... | collective-permute-start | bytes 393224 | tf_op jit(solution)/shard_map/while/body/eval_jaxpr/ppermute | solution.py:18
  449.8 17.7 %copy-start.16 = (f32[512]{0:T(512)S(1)}, f32[512]{0:T(512)}, u32[]{:S(2)}) copy-start(f32[512]{0:T(512)} %broadcast_bitcast_fusion) | copy-start | bytes 6148
  466.4 2.2 slice-start
  469.4 1.2 copy-start.15
  469.4 1.2 copy-start.20
  469.4 1.2 copy-start.21
  469.4 1.2 copy-start.22
  469.4 1.2 copy-start.23
  469.4 1.2 copy-start.24
  469.5 1.2 copy-start.25
  469.5 1.2 copy-start.26
  469.5 1.2 copy-start.27
  469.5 1.2 copy-start.28
  469.5 1.2 copy-start.29
  469.5 1.2 copy-start.30
  469.5 1.2 copy-start.31
  469.5 1.2 copy-start.32
  469.5 1.2 copy-start.33
  469.5 1.2 copy-start.34
  469.6 1.2 copy-start.35
  470.7 2.0 copy-start.19
Sparse Core Ops, SparseCore 0:
  8.9 25.2 all-gather.2
  105.3 176.3 reduce-scatter.2
  283.7 126.0 all-gather.4
  480.0 40.5 reduce-scatter.4
where the time goes:
time: 529 us; the launch traced here: 527 us
  waiting for transfers between devices  285 us (54%)
  other arithmetic  102 us (19%)
  matrix products  49.9 us (9%)
  starting transfers between devices  47.1 us (9%)
  local copies, waits for them, and re-layouts  28.4 us (5%)
  between operations  13.9 us (3%)
    reduce_scatter x1, waiting for transfers between devices, per_device(): lax.psum_scatter(jnp.dot(feature_columns, joined, preferred_element_type=...  159 us
    another operation x2, other arithmetic, block_terms(): jax.scipy.linalg.solve_triangular(system, value_matrix * write_strength_r...  79.4 us
    all_to_all x1, waiting for transfers between devices, per_device(): lax.all_to_all(normed, 'sp', split_axis=1, concat_axis=0, tiled=True)  43.2 us
    ppermute x8, starting transfers between devices, shifted(): lax.ppermute(value, axis, [(source, source + steps) for source in range(l...  41.3 us
    reduce_scatter x1, waiting for transfers between devices, per_device(): lax.psum_scatter(partial_value.astype(jnp.bfloat16), 'tp', scatter_dimens...  40.7 us
    all_gather x1, waiting for transfers between devices, per_device(): gathered = lax.all_gather(inputs, 'tp', axis=1, tiled=True)  24.9 us
    ppermute x8, waiting for transfers between devices, shifted(): lax.ppermute(value, axis, [(source, source + steps) for source in range(l...  17.6 us
  transfers between devices with their start and end apart: 13, of which 11 were waited for; matrix products, arithmetic and copies ran while one was open for 29% of the time, Pallas kernels for 0%

commit v1 on v0

--- a/solution.py
+++ b/solution.py
@@ -6,6 +6,7 @@
 HD = 128
 PC = 128
 BLK = 64
+PAIR = 2
 
 
 epsilon = 1e-06
@@ -74,6 +75,30 @@
     return (query_matrix, incoming_keys, value_matrix, write_strength_rows, decay_log_rows)
 
 
+def unit_lower_inverse(lower_part):
+    size = lower_part.shape[-1]
+    rows, columns = jnp.arange(size)[:, None], jnp.arange(size)[None, :]
+    identity = jnp.eye(size, dtype=jnp.float32)
+    span = 16
+    power = jnp.where(rows // span == columns // span, lower_part, 0.0)
+    inverse = identity - power
+    reach = 2
+    while reach < span:
+        power = jnp.matmul(power, power, precision=highest)
+        inverse = inverse + jnp.matmul(inverse, power, precision=highest)
+        reach *= 2
+    while span < size:
+        across = (rows // span != columns // span) & (
+            rows // (2 * span) == columns // (2 * span)
+        )
+        link = jnp.where(across, lower_part, 0.0)
+        inverse = inverse - jnp.matmul(
+            jnp.matmul(inverse, link, precision=highest), inverse, precision=highest
+        )
+        span *= 2
+    return inverse
+
+
 def block_terms(query_matrix, incoming_keys, value_matrix, write_strength_rows, decay_log_rows):
     length, head_count, head_depth = query_matrix.shape
     blocks = length // BLK
@@ -101,13 +126,13 @@
         jnp.einsum("hnid,hnjd->hnij", weighted, incoming_keys, precision=highest) * decay_table,
         0.0,
     )
-    system = lower_part + jnp.eye(BLK, dtype=jnp.float32)
-    corrected = jax.scipy.linalg.solve_triangular(
-        system, value_matrix * write_strength_rows[..., None], lower=True
-    )
-    erased = jax.scipy.linalg.solve_triangular(
-        system, weighted * jnp.exp(running)[..., None], lower=True
-    )
+    inverse = unit_lower_inverse(lower_part)
+    right_sides = jnp.concatenate(
+        [value_matrix * write_strength_rows[..., None], weighted * jnp.exp(running)[..., None]],
+        axis=-1,
+    )
+    solved = jnp.matmul(inverse, right_sides, precision=highest)
+    corrected, erased = solved[..., :head_depth], solved[..., head_depth:]
     scores = (
         jnp.einsum("hnid,hnjd->hnij", query_matrix, incoming_keys, precision=highest) * decay_table
     )
@@ -224,13 +249,39 @@
     weights = (pooling_input_weight, query_weight, key_weight, value_weight, gate_weight)
     widths = [member.shape[1] for member in weights]
     joined = jnp.concatenate(weights, axis=1)
-    feature_columns = lax.all_to_all(normed, "sp", split_axis=1, concat_axis=0, tiled=True)
-    summed_rows = lax.psum_scatter(
-        jnp.dot(feature_columns, joined, preferred_element_type=jnp.float32).astype(jnp.bfloat16),
-        "sp",
-        scatter_dimension=0,
-        tiled=True,
-    ).astype(jnp.float32)
+    sp_count = lax.axis_size("sp")
+    pairs, outer = PAIR, sp_count // PAIR
+    me = lax.axis_index("sp")
+    mate_weights = lax.ppermute(joined, "sp", [(d, d ^ 1) for d in range(sp_count)])
+    is_odd = (me % pairs) == 1
+    depth = joined.shape[0]
+    my_outer = me // pairs
+
+    def feature_block(which):
+        return lax.dynamic_slice_in_dim(normed, which * (pairs * depth), pairs * depth, 1)
+
+    def outer_shift(value, step):
+        return lax.ppermute(
+            value, "sp", [(d, (d + step * pairs) % sp_count) for d in range(sp_count)]
+        )
+
+    arrived = [feature_block(my_outer)]
+    for step in range(1, outer):
+        arrived.append(outer_shift(feature_block((my_outer + step) % outer), step))
+    returned = []
+    for step in list(range(1, outer)) + [0]:
+        block = arrived[step]
+        mine = jnp.where(is_odd, block[:, depth:], block[:, :depth])
+        other = jnp.where(is_odd, block[:, :depth], block[:, depth:])
+        partial_rows = jnp.dot(mine, joined, preferred_element_type=jnp.float32) + jnp.dot(
+            other, mate_weights, preferred_element_type=jnp.float32
+        )
+        if step:
+            returned.append(outer_shift(partial_rows.astype(jnp.bfloat16), outer - step))
+        else:
+            summed_rows = partial_rows
+    for piece in returned:
+        summed_rows = summed_rows + piece.astype(jnp.float32)
     split_points = [sum(widths[: split_index + 1]) for split_index in range(len(widths) - 1)]
     projected = jnp.split(summed_rows, split_points, axis=1)
     pool_rows, query_row_block, key_matrix_rows, value_row_block, gate_rows = (
@@ -269,31 +320,43 @@
         query_matrix, incoming_keys, value_matrix, write_strength_rows, decay_log_rows
     )
     transition = compose_maps(terms)
-    identity = (
-        jnp.broadcast_to(jnp.eye(HD, dtype=jnp.float32), (head_count, HD, HD)),
-        jnp.zeros((head_count, HD, HD), jnp.float32),
-    )
-
-    def pass_state(step_index, state_now):
-        advanced = (
-            jnp.einsum("hij,hjk->hik", transition[0], state_now, precision=highest) + transition[1]
-        )
-        return shifted(advanced.astype(jnp.bfloat16), "sp", 1).astype(advanced.dtype)
-
-    state_in = lax.fori_loop(0, lax.axis_size("sp") - 1, pass_state, identity[1])
+    packed = jnp.stack(transition).astype(jnp.bfloat16)
+    mate_map = lax.ppermute(packed, "sp", [(d, d ^ 1) for d in range(sp_count)]).astype(
+        jnp.float32
+    )
+    first = jnp.where(is_odd, mate_map, jnp.stack(transition))
+    second = jnp.where(is_odd, jnp.stack(transition), mate_map)
+    joint_move = jnp.matmul(second[0], first[0], precision=highest)
+    joint_add = jnp.matmul(second[0], first[1], precision=highest) + second[1]
+    state_in = jnp.zeros_like(joint_add)
+    for hop in range(outer - 1):
+        advanced = joint_add
+        if hop:
+            advanced = jnp.matmul(joint_move, state_in, precision=highest) + joint_add
+        state_in = shifted(advanced.astype(jnp.bfloat16), "sp", pairs).astype(jnp.float32)
+    after_first = jnp.matmul(first[0], state_in, precision=highest) + first[1]
+    state_in = jnp.where(is_odd, after_first, state_in)
     unused_state, outputs = run_blocks(state_in, terms)
     delta_out = delta_finish(outputs, gate_rows, head_norm_gain)
     both_out = jnp.concatenate([pool_out, delta_out], axis=1)
     out_weights = jnp.concatenate([pooling_output_weight, delta_output_weight], axis=0)
-    partial_value = jnp.dot(
-        both_out,
-        lax.all_gather(out_weights, "sp", axis=1, tiled=True),
-        preferred_element_type=jnp.float32,
-    )
-    summed = lax.psum_scatter(
-        partial_value.astype(jnp.bfloat16), "tp", scatter_dimension=1, tiled=True
-    )
-    return summed
+    full_weights = lax.all_gather(out_weights, "sp", axis=1, tiled=True)
+    tp_count = lax.axis_size("tp")
+    my_tp = lax.axis_index("tp")
+    width = full_weights.shape[1] // tp_count
+    sent = []
+    for step in list(range(1, tp_count)) + [0]:
+        columns = lax.dynamic_slice_in_dim(
+            full_weights, ((my_tp + step) % tp_count) * width, width, 1
+        )
+        part = jnp.dot(both_out, columns, preferred_element_type=jnp.float32).astype(jnp.bfloat16)
+        if step:
+            part = lax.ppermute(
+                part, "tp", [(d, (d + step) % tp_count) for d in range(tp_count)]
+            )
+        sent.append(part)
+    summed = sum(part.astype(jnp.float32) for part in sent)
+    return summed.astype(jnp.bfloat16)
 
 
 def solution(mesh):

time: 529 us -> 427 us (0.81)
  waiting for transfers between devices: 285 us -> 169 us
  starting transfers between devices: 47.1 us -> 133 us
  other arithmetic: 102 us -> 21.8 us
  matrix products: 49.9 us -> 69.3 us
  local copies, waits for them, and re-layouts: 28.4 us -> 15.2 us
    reduce_scatter x2 -> x0, waiting for transfers between devices: 200 us -> none  [the longest x1 159 us: per_device(): lax.psum_scatter(jnp.dot(feature_columns, joined, preferred_element_type=...]
    ppermute x0 -> x11, waiting for transfers between devices: none -> 151 us  [the longest x6 94.9 us: outer_shift(): lax.ppermute(value, 'sp', [(d, (d + step * pairs) % sp_count) for d in ra...]
    ppermute x0 -> x11, starting transfers between devices: none -> 117 us  [the longest x6 89.5 us: outer_shift(): lax.ppermute(value, 'sp', [(d, (d + step * pairs) % sp_count) for d in ra...]
    another operation x2 -> x0, other arithmetic: 79.4 us -> none  [block_terms(): jax.scipy.linalg.solve_triangular(system, value_matrix * write_strength_r...]
    all_to_all x1 -> x0, waiting for transfers between devices: 43.2 us -> none  [per_device(): lax.all_to_all(normed, 'sp', split_axis=1, concat_axis=0, tiled=True)]
    ppermute x8 -> x4, starting transfers between devices: 41.3 us -> 16 us  [shifted(): lax.ppermute(value, axis, [(source, source + steps) for source in range(l...]
    dot_general x9 -> x28, matrix products: 20.1 us -> 40.4 us  [the longest x4 12.1 us: per_device(): jnp.dot(other, mate_weights, preferred_element_type=jnp.float32)]
    ppermute x8 -> x4, waiting for transfers between devices: 17.6 us -> 3.5 us  [shifted(): lax.ppermute(value, axis, [(source, source + steps) for source in range(l...]
  transfers between devices with their start and end apart: 13 -> 17, of which waited for: 11 -> 10; matrix products, arithmetic and copies ran while one was open for 29% -> 24% of each run, Pallas kernels for 0% -> 0%
where the time goes in v1:
time: 427 us; the launch traced here: 424 us
  waiting for transfers between devices  169 us (40%)
  starting transfers between devices  133 us (31%)
  matrix products  69.3 us (16%)
  other arithmetic  21.8 us (5%)
  local copies, waits for them, and re-layouts  15.2 us (4%)
  between operations  14.7 us (3%)
    ppermute x6, waiting for transfers between devices, outer_shift(): lax.ppermute(value, 'sp', [(d, (d + step * pairs) % sp_count) for d in ra...  94.9 us
    ppermute x6, starting transfers between devices, outer_shift(): lax.ppermute(value, 'sp', [(d, (d + step * pairs) % sp_count) for d in ra...  89.5 us
    ppermute x1, waiting for transfers between devices, per_device(): lax.ppermute(joined, 'sp', [(d, d ^ 1) for d in range(sp_count)])  36.9 us
    ppermute x1, starting transfers between devices, per_device(): lax.ppermute(packed, 'sp', [(d, d ^ 1) for d in range(sp_count)])  22.5 us
    ppermute x4, starting transfers between devices, shifted(): lax.ppermute(value, axis, [(source, source + steps) for source in range(l...  16 us
    ppermute x3, waiting for transfers between devices, per_device(): lax.ppermute(part, 'tp', [(d, (d + step) % tp_count) for d in range(tp_co...  15.5 us
    all_gather x1, waiting for transfers between devices, per_device(): gathered = lax.all_gather(inputs, 'tp', axis=1, tiled=True)  13.9 us
    dot_general x4, matrix products, per_device(): jnp.dot(other, mate_weights, preferred_element_type=jnp.float32)  12.1 us
  transfers between devices with their start and end apart: 17, of which 10 were waited for; matrix products, arithmetic and copies ran while one was open for 24% of the time, Pallas kernels for 0%

profile of v1, /device:TPU:0, one launch (start us, length us, event | category | flops | bytes accessed | tf_op | source)
XLA Modules:
  0.0 423.6 jit_solution(4522720732244237390)
XLA Ops:
  7.3 1.2 constant_dynamic-update-slice_fusion.4
  8.6 1.1 constant_dynamic-update-slice_fusion.3
  9.8 3.1 collective-permute-start
  12.9 1.1 pad_maximum_fusion
  20.3 13.9 %all-gather.3.cloned.1.call-done = bf16[256,4096]{1,0:T(8,128)(2,1)} async-done(((bf16[256,1024]{1,0:T(8,128)(2,1)}), bf16[256,4096]{1,0:T(8,128)(2,1)}) %all-gather.3.cloned.1.call-update) | async-done | bytes 2097168 | tf_op jit(solution)/shard_map/all_gather | solution.py:230
  34.2 2.2 fusion.25
  37.3 1.5 collective-permute-start.1
  40.3 2.5 collective-permute-start.3
  42.7 1.4 collective-permute-start.5
  44.2 36.9 %collective-permute-done = bf16[512,2560]{1,0:T(8,128)(2,1)} collective-permute-done((bf16[512,2560]{1,0:T(8,128)(2,1)S(1)}, bf16[512,2560]{1,0:T(8,128)(2,1)}, u32[]{:S(2)}, u32[]{:S(2)}) %collective-permute-start) | collective-permute-done | bytes 2621472 | tf_op jit(solution)/shard_map/ppermute | solution.py:255
  81.1 2.6 fusion.178
  83.7 1.9 fusion.32
  85.6 3.8 collective-permute-start.2
  89.5 8.8 %collective-permute-done.3 = bf16[256,1024]{1,0:T(8,128)(2,1)S(1)} collective-permute-done((bf16[256,1024]{1,0:T(8,128)(2,1)S(1)}, bf16[256,1024]{1,0:T(8,128)(2,1)S(1)}, u32[]{:S(2)}, u32[]{:S(2)}) %collective-permute-start.3) | collective-permute-done | bytes 524320 | tf_op jit(solution)/shard_map/ppermute | solution.py:264
  98.2 2.6 fusion.175
  100.8 1.9 fusion.33
  102.8 2.6 fusion.172
  105.4 1.9 fusion.34
  107.3 80.3 %collective-permute-start.6 = (bf16[256,2560]{1,0:T(8,128)(2,1)}, bf16[256,2560]{1,0:T(8,128)(2,1)}, u32[]{:S(2)}, u32[]{:S(2)}) collective-permute-start(bf16[256,2560]{1,0:T(8,128)(2,1)} %fusion.34), channel_id=1, source_target_pairs={{0,8},{4,12},{8,16},{12,20},{16,24},{20,28},{24,0},{28,4},{1,9},{5... | collective-permute-start | bytes 3932168 | tf_op jit(solution)/shard_map/ppermute | solution.py:264
  188.3 2.3 fusion.213
  194.5 1.9 fusion.182
  196.4 86.2 %collective-permute-done.6 = bf16[256,2560]{1,0:T(8,128)(2,1)} collective-permute-done((bf16[256,2560]{1,0:T(8,128)(2,1)}, bf16[256,2560]{1,0:T(8,128)(2,1)}, u32[]{:S(2)}, u32[]{:S(2)}) %collective-permute-start.6) | collective-permute-done | bytes 1310752 | tf_op jit(solution)/shard_map/ppermute | solution.py:264
  282.5 4.3 %fusion.31 = bf16[256,2560]{1,0:T(8,128)(2,1)S(1)} fusion(f32[256,2560]{1,0:T(8,128)S(1)} %fusion.182, bf16[512,2560]{1,0:T(8,128)(2,1)} %collective-permute-done, bf16[256,2560]{1,0:T(8,128)(2,1)} %collective-permute-done.6, bf16[256,2560]{1,0:T(8,128)(2,1)} %collective-permute-done.4, bf16[256,2560]{1,0:T(8,128)(2,1)} %collective-permute-done.2, ...), kind=kOutput, calls=%fused_computation.45 | convolution fusion | flops 676462592 | bytes 11010057 | tf_op jit(solution)/shard_map/dot_general | solution.py:276
  287.9 1.3 fusion.245
  289.2 3.4 collective-permute-start.7
  293.3 1.2 reshape.517
  295.2 1.4 multiply_multiply_fusion
  296.7 1.0 fusion.58
  298.5 1.0 reshape.519
  300.8 1.4 convolution_add_fusion.9
  306.2 1.0 fusion.63
  308.4 5.2 %while.22 = (s32[]{:T(128)}, f32[4,128,256]{2,1,0:T(8,128)S(1)}, f32[4,4]{1,0:T(4,128)S(1)}, f32[4,4,64,128]{3,2,1,0:T(8,128)S(1)}, f32[4,4,64,128]{3,2,1,0:T(8,...) while((s32[]{:T(128)}, f32[4,128,256]{2,1,0:T(8,128)S(1)}, f32[4,4]{1,0:T(4,128)S(1)}, ...), condition=%wide.region_4.5_spmd, body=%wide.region_3.4_spmd.sunk | while | flops 201654272 | bytes 2753149 | solution.py:191
  313.6 2.2 bitcast_multiply_fusion.18
  315.8 2.9 fusion.59
  318.7 22.5 %collective-permute-start.8 = (bf16[2,4,128,128]{3,2,1,0:T(8,128)(2,1)S(1)}, bf16[2,4,128,128]{3,2,1,0:T(8,128)(2,1)S(1)}, u32[]{:S(2)}, u32[]{:S(2)}) collective-permute-start(bf16[2,4,128,128]{3,2,1,0:T(8,128)(2,1)S(1)} %fusion.146), channel_id=1, source_target_pairs={{0,4},{4,0},{8,12},{12,8},{16,20},{20,16},{24,28},{28,24},{1,5},{5... | collective-permute-start | bytes 786440 | tf_op jit(solution)/shard_map/ppermute | solution.py:324
  342.1 1.0 slice_bitcast_fusion.17
  343.2 3.6 collective-permute-done.8
  347.3 4.4 %collective-permute-start.9 = (bf16[4,128,128]{2,1,0:T(8,128)(2,1)S(1)}, bf16[4,128,128]{2,1,0:T(8,128)(2,1)S(1)}, u32[]{:S(2)}, u32[]{:S(2)}) collective-permute-start(bf16[4,128,128]{2,1,0:T(8,128)(2,1)S(1)} %get-tuple-element.231), channel_id=1, source_target_pairs={{0,8},{4,12},{8,16},{12,20},{16,24},{20,28},{1,9},{5,13},{9,17},{1... | collective-permute-start | bytes 393224 | tf_op jit(solution)/shard_map/ppermute | solution.py:19
  352.1 2.1 collective-permute-done.9
  354.5 4.4 %collective-permute-start.10 = (bf16[4,128,128]{2,1,0:T(8,128)(2,1)S(1)}, bf16[4,128,128]{2,1,0:T(8,128)(2,1)S(1)}, u32[]{:S(2)}, u32[]{:S(2)}) collective-permute-start(bf16[4,128,128]{2,1,0:T(8,128)(2,1)S(1)} %fusion.61), channel_id=1, source_target_pairs={{0,8},{4,12},{8,16},{12,20},{16,24},{20,28},{1,9},{5,13},{9,17},{1... | collective-permute-start | bytes 393224 | tf_op jit(solution)/shard_map/ppermute | solution.py:19
  359.0 1.8 fusion.85
  360.8 1.0 copy.212
  362.1 3.9 collective-permute-start.11
  366.0 1.1 multiply_convert_fusion
  367.1 1.4 collective-permute-done.11
  368.8 16.5 %while.23 = (s32[]{:T(128)}, f32[4,128,128]{2,1,0:T(8,128)S(1)}, f32[4,4,64,128]{3,2,1,0:T(8,128)}, f32[4,4]{1,0:T(4,128)S(1)}, f32[4,4,64,128]{3,2,1,0:T(8,128)...) while((s32[]{:T(128)}, f32[4,128,128]{2,1,0:T(8,128)S(1)}, ...), condition=%wide.region_7.8_spmd, body=%wide.region_6.7_spmd.sunk | while | flops 176357376 | bytes 2493581 | solution.py:159
  369.1 1.2 fusion.318
  370.3 1.9 fusion.319
  373.2 1.2 fusion.318
  374.4 1.9 fusion.319
  377.4 1.2 fusion.318
  378.5 1.9 fusion.319
  381.5 1.2 fusion.318
  382.7 1.9 fusion.319
  385.2 1.3 multiply_reduce_fusion
  386.6 1.4 copy.208
  388.6 2.3 fusion.43
  391.0 2.3 fusion.46
  393.4 3.1 fusion.49
  396.5 1.7 collective-permute-start.14
  398.2 4.0 collective-permute-done.12
  402.2 5.9 %collective-permute-done.13 = bf16[256,1024]{1,0:T(8,128)(2,1)S(1)} collective-permute-done((bf16[256,1024]{1,0:T(8,128)(2,1)S(1)}, bf16[256,1024]{1,0:T(8,128)(2,1)S(1)}, u32[]{:S(2)}, u32[]{:S(2)}) %collective-permute-start.13) | collective-permute-done | bytes 524320 | tf_op jit(solution)/shard_map/ppermute | solution.py:354
  408.2 5.5 %collective-permute-done.14 = bf16[256,1024]{1,0:T(8,128)(2,1)S(1)} collective-permute-done((bf16[256,1024]{1,0:T(8,128)(2,1)}, bf16[256,1024]{1,0:T(8,128)(2,1)S(1)}, u32[]{:S(2)}, u32[]{:S(2)}) %collective-permute-start.14) | collective-permute-done | bytes 524320 | tf_op jit(solution)/shard_map/ppermute | solution.py:354
  413.7 3.1 add_convert_fusion
  (213 shorter events, 35.5 us)
Async XLA Ops:
  6.5 352.3 %copy-start = (bf16[4,128,128]{2,1,0:T(8,128)(2,1)S(1)}, bf16[4,128,128]{2,1,0:T(8,128)(2,1)}, u32[]{:S(2)}) copy-start(bf16[4,128,128]{2,1,0:T(8,128)(2,1)} %param.32) | copy-start | bytes 393220
  6.5 3.1 copy-start.7
  6.5 27.7 %all-gather.3.cloned.1.call-start = ((), (), s32[]{:S(2)}) async-start(), calls=%async_computation | async-start | bytes 2621440 | tf_op jit(solution)/shard_map/all_gather | solution.py:230
  7.3 381.3 %all-gather.5.cloned.1.call-start = ((), (), s32[]{:S(2)}) async-start(), calls=%async_computation.1 | async-start | bytes 9437184 | tf_op jit(solution)/shard_map/all_gather | solution.py:343
  7.3 2.4 copy-start.8
  7.3 2.5 copy-start.9
  7.3 5.6 %copy-start.10 = (bf16[512,512]{1,0:T(8,128)(2,1)S(1)}, bf16[512,512]{1,0:T(8,128)(2,1)}, u32[]{:S(2)}) copy-start(bf16[512,512]{1,0:T(8,128)(2,1)} %param.41) | copy-start | bytes 1572868
  7.3 5.6 %copy-start.11 = (bf16[512,512]{1,0:T(8,128)(2,1)S(1)}, bf16[512,512]{1,0:T(8,128)(2,1)}, u32[]{:S(2)}) copy-start(bf16[512,512]{1,0:T(8,128)(2,1)} %param.40) | copy-start | bytes 1572868
  9.7 8.6 %copy-start.20 = (bf16[4096]{0:T(1024)(128)(2,1)S(1)}, bf16[4096]{0:T(1024)(128)(2,1)}, u32[]{:S(2)}) copy-start(bf16[4096]{0:T(1024)(128)(2,1)} %param.24) | copy-start | bytes 24580
  9.7 8.7 %copy-start.42 = (f32[128]{0:T(128)S(1)}, f32[128]{0:T(128)}, u32[]{:S(2)}) copy-start(f32[128]{0:T(128)} %param.39) | copy-start | bytes 1540
  9.7 9.9 %copy-start.45 = (f32[4]{0:T(128)S(1)}, f32[4]{0:T(128)}, u32[]{:S(2)}) copy-start(f32[4]{0:T(128)} %param.34) | copy-start | bytes 52
  9.8 71.3 %collective-permute-start = (bf16[512,2560]{1,0:T(8,128)(2,1)S(1)}, bf16[512,2560]{1,0:T(8,128)(2,1)}, u32[]{:S(2)}, u32[]{:S(2)}) collective-permute-start(bf16[512,2560]{1,0:T(8,128)(2,1)S(1)} %constant_dynamic-update-slice_fusion), channel_id=1, source_target_pairs={{0,4},{4,0},{8,12},{12,8},{16,20},{20,16},{24,28},{28,24},{1,5},{5... | collective-permute-start | bytes 7864328 | tf_op jit(solution)/shard_map/ppermute | solution.py:255
  18.3 278.4 %copy-start.14 = (pred[64,64]{1,0:T(8,128)(4,1)}, pred[64,64]{1,0:T(8,128)(4,1)S(1)}, u32[]{:S(2)}) copy-start(pred[64,64]{1,0:T(8,128)(4,1)S(1)} %get-tuple-element.253) | copy-start | bytes 12292
  34.2 2.2 copy-start.2
  37.1 46.6 %copy-start.1 = (bf16[256,4096]{1,0:T(8,128)(2,1)}, bf16[256,4096]{1,0:T(8,128)(2,1)S(1)}, u32[]{:S(2)}) copy-start(bf16[256,4096]{1,0:T(8,128)(2,1)S(1)} %fusion.27) | copy-start | bytes 6291460
  37.3 43.9 %collective-permute-start.1 = (bf16[256,1024]{1,0:T(8,128)(2,1)S(1)}, bf16[256,1024]{1,0:T(8,128)(2,1)S(1)}, u32[]{:S(2)}, u32[]{:S(2)}) collective-permute-start(bf16[256,1024]{1,0:T(8,128)(2,1)S(1)} %get-tuple-element.193), channel_id=1, source_target_pairs={{0,8},{4,12},{8,16},{12,20},{16,24},{20,28},{24,0},{28,4},{1,9},{5... | collective-permute-start | bytes 1572872 | tf_op jit(solution)/shard_map/ppermute | solution.py:264
  40.3 58.0 %collective-permute-start.3 = (bf16[256,1024]{1,0:T(8,128)(2,1)S(1)}, bf16[256,1024]{1,0:T(8,128)(2,1)S(1)}, u32[]{:S(2)}, u32[]{:S(2)}) collective-permute-start(bf16[256,1024]{1,0:T(8,128)(2,1)S(1)} %get-tuple-element.195), channel_id=1, source_target_pairs={{0,16},{4,20},{8,24},{12,28},{16,0},{20,4},{24,8},{28,12},{1,17},{... | collective-permute-start | bytes 1572872 | tf_op jit(solution)/shard_map/ppermute | solution.py:264
  42.7 60.0 %collective-permute-start.5 = (bf16[256,1024]{1,0:T(8,128)(2,1)S(1)}, bf16[256,1024]{1,0:T(8,128)(2,1)S(1)}, u32[]{:S(2)}, u32[]{:S(2)}) collective-permute-start(bf16[256,1024]{1,0:T(8,128)(2,1)S(1)} %get-tuple-element.194), channel_id=1, source_target_pairs={{0,24},{4,28},{8,0},{12,4},{16,8},{20,12},{24,16},{28,20},{1,25},{... | collective-permute-start | bytes 1572872 | tf_op jit(solution)/shard_map/ppermute | solution.py:264
  85.6 110.7 %collective-permute-start.2 = (bf16[256,2560]{1,0:T(8,128)(2,1)}, bf16[256,2560]{1,0:T(8,128)(2,1)}, u32[]{:S(2)}, u32[]{:S(2)}) collective-permute-start(bf16[256,2560]{1,0:T(8,128)(2,1)} %fusion.32), channel_id=1, source_target_pairs={{0,24},{4,28},{8,0},{12,4},{16,8},{20,12},{24,16},{28,20},{1,25},{... | collective-permute-start | bytes 3932168 | tf_op jit(solution)/shard_map/ppermute | solution.py:264
  102.8 93.6 %collective-permute-start.4 = (bf16[256,2560]{1,0:T(8,128)(2,1)}, bf16[256,2560]{1,0:T(8,128)(2,1)}, u32[]{:S(2)}, u32[]{:S(2)}) collective-permute-start(bf16[256,2560]{1,0:T(8,128)(2,1)} %fusion.33), channel_id=1, source_target_pairs={{0,16},{4,20},{8,24},{12,28},{16,0},{20,4},{24,8},{28,12},{1,17},{... | collective-permute-start | bytes 3932168 | tf_op jit(solution)/shard_map/ppermute | solution.py:264
  107.3 83.2 %copy-start.22 = (f32[256,4]{0,1:T(4,128)S(1)}, f32[256,4]{0,1:T(4,128)}, u32[]{:S(2)}) copy-start(f32[256,4]{0,1:T(4,128)} %param.38) | copy-start | bytes 12292
  107.3 83.2 %copy-start.23 = (f32[256,4]{0,1:T(4,128)S(1)}, f32[256,4]{0,1:T(4,128)}, u32[]{:S(2)}) copy-start(f32[256,4]{0,1:T(4,128)} %param.37) | copy-start | bytes 12292
  107.3 83.2 %copy-start.43 = (f32[4]{0:T(128)S(1)}, f32[4]{0:T(128)}, u32[]{:S(2)}) copy-start(f32[4]{0:T(128)} %param.36) | copy-start | bytes 52
  107.3 83.2 %copy-start.44 = (f32[4]{0:T(128)S(1)}, f32[4]{0:T(128)}, u32[]{:S(2)}) copy-start(f32[4]{0:T(128)} %param.35) | copy-start | bytes 52
  107.3 175.2 %collective-permute-start.6 = (bf16[256,2560]{1,0:T(8,128)(2,1)}, bf16[256,2560]{1,0:T(8,128)(2,1)}, u32[]{:S(2)}, u32[]{:S(2)}) collective-permute-start(bf16[256,2560]{1,0:T(8,128)(2,1)} %fusion.34), channel_id=1, source_target_pairs={{0,8},{4,12},{8,16},{12,20},{16,24},{20,28},{24,0},{28,4},{1,9},{5... | collective-permute-start | bytes 3932168 | tf_op jit(solution)/shard_map/ppermute | solution.py:264
  286.8 1.1 copy-start.3
  289.2 52.0 %collective-permute-start.7 = (bf16[16,512]{1,0:T(8,128)(2,1)}, bf16[16,512]{1,0:T(8,128)(2,1)}, u32[]{:S(2)}, u32[]{:S(2)}) collective-permute-start(bf16[16,512]{1,0:T(8,128)(2,1)} %slice.227), channel_id=1, source_target_pairs={{0,4},{4,8},{8,12},{12,16},{16,20},{20,24},{24,28},{1,5},{5,9},{9,... | collective-permute-start | bytes 49160 | tf_op jit(solution)/shard_map/ppermute | solution.py:19
  300.8 2.8 copy-start.13
  302.9 2.0 copy-start.12
  304.2 2.0 copy-start.5
  304.2 2.0 copy-start.6
  307.2 0.7 copy-start.17
  307.4 0.9 copy-start.25
  308.3 5.3 %copy-start.16 = (f32[4,4,64]{2,1,0:T(4,128)S(1)}, f32[4,4,64]{2,1,0:T(4,128)}, u32[]{:S(2)}) copy-start(f32[4,4,64]{2,1,0:T(4,128)} %copy.200) | copy-start | bytes 12292
  308.3 7.5 %copy-start.15 = (pred[64,64]{1,0:T(8,128)(4,1)S(1)}, pred[64,64]{1,0:T(8,128)(4,1)}, u32[]{:S(2)}) copy-start(pred[64,64]{1,0:T(8,128)(4,1)} %copy-done.14) | copy-start | bytes 12292
  308.4 7.5 %copy-start.21 = (f32[4,4,64]{2,1,0:T(4,128)S(1)}, f32[4,4,64]{2,1,0:T(4,128)}, u32[]{:S(2)}) copy-start(f32[4,4,64]{2,1,0:T(4,128)} %copy.202) | copy-start | bytes 12292
  313.6 27.7 %slice-start = ((bf16[256,2560]{1,0:T(8,128)(2,1)}), bf16[256,512]{1,0:T(8,128)(2,1)S(1)}, s32[]{:S(2)}) async-start(bf16[256,2560]{1,0:T(8,128)(2,1)} %copy-done.3), calls=%async_computation.2 | async-start | bytes 524288 | tf_op jit(solution)/shard_map/split | solution.py:286
  318.7 28.1 %collective-permute-start.8 = (bf16[2,4,128,128]{3,2,1,0:T(8,128)(2,1)S(1)}, bf16[2,4,128,128]{3,2,1,0:T(8,128)(2,1)S(1)}, u32[]{:S(2)}, u32[]{:S(2)}) collective-permute-start(bf16[2,4,128,128]{3,2,1,0:T(8,128)(2,1)S(1)} %fusion.146), channel_id=1, source_target_pairs={{0,4},{4,0},{8,12},{12,8},{16,20},{20,16},{24,28},{28,24},{1,5},{5... | collective-permute-start | bytes 786440 | tf_op jit(solution)/shard_map/ppermute | solution.py:324
  343.1 15.8 %copy-start.18 = (f32[256,4]{0,1:T(4,128)S(1)}, f32[256,4]{0,1:T(4,128)}, u32[]{:S(2)}) copy-start(f32[256,4]{0,1:T(4,128)} %minimum_convert_fusion) | copy-start | bytes 12292
  343.1 15.8 %copy-start.26 = (f32[4]{0:T(128)S(1)}, f32[4]{0:T(128)}, u32[]{:S(2)}) copy-start(f32[4]{0:T(128)} %get-tuple-element.235) | copy-start | bytes 52
  343.1 15.8 %copy-start.27 = (f32[4]{0:T(128)S(1)}, f32[4]{0:T(128)}, u32[]{:S(2)}) copy-start(f32[4]{0:T(128)} %get-tuple-element.236) | copy-start | bytes 52
  343.1 15.8 %copy-start.28 = (f32[4]{0:T(128)S(1)}, f32[4]{0:T(128)}, u32[]{:S(2)}) copy-start(f32[4]{0:T(128)} %get-tuple-element.237) | copy-start | bytes 52
  343.1 15.8 %copy-start.29 = (f32[4]{0:T(128)S(1)}, f32[4]{0:T(128)}, u32[]{:S(2)}) copy-start(f32[4]{0:T(128)} %get-tuple-element.238) | copy-start | bytes 52
  343.1 15.8 %copy-start.30 = (f32[4]{0:T(128)S(1)}, f32[4]{0:T(128)}, u32[]{:S(2)}) copy-start(f32[4]{0:T(128)} %get-tuple-element.239) | copy-start | bytes 52
  343.1 15.8 %copy-start.31 = (f32[4]{0:T(128)S(1)}, f32[4]{0:T(128)}, u32[]{:S(2)}) copy-start(f32[4]{0:T(128)} %get-tuple-element.240) | copy-start | bytes 52
  343.1 15.8 %copy-start.32 = (f32[4]{0:T(128)S(1)}, f32[4]{0:T(128)}, u32[]{:S(2)}) copy-start(f32[4]{0:T(128)} %get-tuple-element.241) | copy-start | bytes 52
  343.1 15.8 %copy-start.33 = (f32[4]{0:T(128)S(1)}, f32[4]{0:T(128)}, u32[]{:S(2)}) copy-start(f32[4]{0:T(128)} %get-tuple-element.242) | copy-start | bytes 52
  343.2 15.8 %copy-start.34 = (f32[4]{0:T(128)S(1)}, f32[4]{0:T(128)}, u32[]{:S(2)}) copy-start(f32[4]{0:T(128)} %get-tuple-element.243) | copy-start | bytes 52
  343.2 15.8 %copy-start.35 = (f32[4]{0:T(128)S(1)}, f32[4]{0:T(128)}, u32[]{:S(2)}) copy-start(f32[4]{0:T(128)} %get-tuple-element.244) | copy-start | bytes 52
  343.2 15.8 %copy-start.36 = (f32[4]{0:T(128)S(1)}, f32[4]{0:T(128)}, u32[]{:S(2)}) copy-start(f32[4]{0:T(128)} %get-tuple-element.245) | copy-start | bytes 52
  343.2 15.8 %copy-start.37 = (f32[4]{0:T(128)S(1)}, f32[4]{0:T(128)}, u32[]{:S(2)}) copy-start(f32[4]{0:T(128)} %get-tuple-element.246) | copy-start | bytes 52
  343.2 15.8 %copy-start.38 = (f32[4]{0:T(128)S(1)}, f32[4]{0:T(128)}, u32[]{:S(2)}) copy-start(f32[4]{0:T(128)} %get-tuple-element.247) | copy-start | bytes 52
  343.2 15.8 %copy-start.39 = (f32[4]{0:T(128)S(1)}, f32[4]{0:T(128)}, u32[]{:S(2)}) copy-start(f32[4]{0:T(128)} %get-tuple-element.248) | copy-start | bytes 52
  343.2 15.8 %copy-start.40 = (f32[4]{0:T(128)S(1)}, f32[4]{0:T(128)}, u32[]{:S(2)}) copy-start(f32[4]{0:T(128)} %get-tuple-element.249) | copy-start | bytes 52
  343.2 15.8 %copy-start.41 = (f32[4]{0:T(128)S(1)}, f32[4]{0:T(128)}, u32[]{:S(2)}) copy-start(f32[4]{0:T(128)} %get-tuple-element.250) | copy-start | bytes 52
  347.3 6.9 %collective-permute-start.9 = (bf16[4,128,128]{2,1,0:T(8,128)(2,1)S(1)}, bf16[4,128,128]{2,1,0:T(8,128)(2,1)S(1)}, u32[]{:S(2)}, u32[]{:S(2)}) collective-permute-start(bf16[4,128,128]{2,1,0:T(8,128)(2,1)S(1)} %get-tuple-element.231), channel_id=1, source_target_pairs={{0,8},{4,12},{8,16},{12,20},{16,24},{20,28},{1,9},{5,13},{9,17},{1... | collective-permute-start | bytes 393224 | tf_op jit(solution)/shard_map/ppermute | solution.py:19
  354.5 7.4 %collective-permute-start.10 = (bf16[4,128,128]{2,1,0:T(8,128)(2,1)S(1)}, bf16[4,128,128]{2,1,0:T(8,128)(2,1)S(1)}, u32[]{:S(2)}, u32[]{:S(2)}) collective-permute-start(bf16[4,128,128]{2,1,0:T(8,128)(2,1)S(1)} %fusion.61), channel_id=1, source_target_pairs={{0,8},{4,12},{8,16},{12,20},{16,24},{20,28},{1,9},{5,13},{9,17},{1... | collective-permute-start | bytes 393224 | tf_op jit(solution)/shard_map/ppermute | solution.py:19
  359.0 6.9 %copy-start.24 = (f32[512]{0:T(512)S(1)}, f32[512]{0:T(512)}, u32[]{:S(2)}) copy-start(f32[512]{0:T(512)} %param.33) | copy-start | bytes 6148
  362.1 6.4 %collective-permute-start.11 = (bf16[4,128,128]{2,1,0:T(8,128)(2,1)S(1)}, bf16[4,128,128]{2,1,0:T(8,128)(2,1)S(1)}, u32[]{:S(2)}, u32[]{:S(2)}) collective-permute-start(bf16[4,128,128]{2,1,0:T(8,128)(2,1)S(1)} %fusion.62), channel_id=1, source_target_pairs={{0,8},{4,12},{8,16},{12,20},{16,24},{20,28},{1,9},{5,13},{9,17},{1... | collective-permute-start | bytes 393224 | tf_op jit(solution)/shard_map/ppermute | solution.py:19
  368.7 19.6 %copy-start.4 = (bf16[256,2560]{1,0:T(8,128)(2,1)S(1)}, bf16[256,2560]{1,0:T(8,128)(2,1)}, u32[]{:S(2)}) copy-start(bf16[256,2560]{1,0:T(8,128)(2,1)} %copy-done.3) | copy-start | bytes 3932164
  368.8 19.6 %copy-start.19 = (f32[512]{0:T(512)S(1)}, f32[512]{0:T(512)}, u32[]{:S(2)}) copy-start(f32[512]{0:T(512)} %broadcast_bitcast_fusion) | copy-start | bytes 6148
  390.9 11.3 %collective-permute-start.12 = (bf16[256,1024]{1,0:T(8,128)(2,1)S(1)}, bf16[256,1024]{1,0:T(8,128)(2,1)S(1)}, u32[]{:S(2)}, u32[]{:S(2)}) collective-permute-start(bf16[256,1024]{1,0:T(8,128)(2,1)S(1)} %fusion.43), channel_id=1, source_target_pairs={{0,1},{1,2},{2,3},{3,0},{4,5},{5,6},{6,7},{7,4},{8,9},{9,10},{10,1... | collective-permute-start | bytes 1572872 | tf_op jit(solution)/shard_map/ppermute | solution.py:354
  393.3 14.9 %collective-permute-start.13 = (bf16[256,1024]{1,0:T(8,128)(2,1)S(1)}, bf16[256,1024]{1,0:T(8,128)(2,1)S(1)}, u32[]{:S(2)}, u32[]{:S(2)}) collective-permute-start(bf16[256,1024]{1,0:T(8,128)(2,1)S(1)} %fusion.46), channel_id=1, source_target_pairs={{0,2},{1,3},{2,0},{3,1},{4,6},{5,7},{6,4},{7,5},{8,10},{9,11},{10,... | collective-permute-start | bytes 1572872 | tf_op jit(solution)/shard_map/ppermute | solution.py:354
  396.5 17.2 %collective-permute-start.14 = (bf16[256,1024]{1,0:T(8,128)(2,1)}, bf16[256,1024]{1,0:T(8,128)(2,1)S(1)}, u32[]{:S(2)}, u32[]{:S(2)}) collective-permute-start(bf16[256,1024]{1,0:T(8,128)(2,1)} %fusion.49), channel_id=1, source_target_pairs={{0,3},{1,0},{2,1},{3,2},{4,7},{5,4},{6,5},{7,6},{8,11},{9,8},{10,9... | collective-permute-start | bytes 1572872 | tf_op jit(solution)/shard_map/ppermute | solution.py:354
Sparse Core Ops, SparseCore 0:
  8.9 25.2 all-gather.2
  36.3 269.0 all-gather.4

commit v2 on v1

--- a/solution.py
+++ b/solution.py
@@ -10,7 +10,7 @@
 
 
 epsilon = 1e-06
-highest = lax.Precision.HIGHEST
+highest = lax.Precision.HIGH
 
 
 def shifted(value, axis, steps):
@@ -156,7 +156,7 @@
         return (state_now, output)
 
     stacked = tuple((jnp.moveaxis(member, 1, 0) for member in terms))
-    final_state, outputs = lax.scan(advance, state_start, stacked)
+    final_state, outputs = lax.scan(advance, state_start, stacked, unroll=True)
     blocks, head_count, block_rows, head_depth = outputs.shape
     return (
         final_state,
@@ -188,7 +188,7 @@
     stacked = tuple(
         (jnp.moveaxis(member, 1, 0) for member in (corrected, erased, key_decayed, block_total))
     )
-    joined_map, unused = lax.scan(absorb, start_map, stacked)
+    joined_map, unused = lax.scan(absorb, start_map, stacked, unroll=True)
     return (joined_map[..., :head_depth], joined_map[..., head_depth:])
 
 
@@ -227,7 +227,41 @@
     delta_output_weight,
 ):
     tok_rows = inputs.shape[0]
-    gathered = lax.all_gather(inputs, "tp", axis=1, tiled=True)
+    sp_count, tp_count = lax.axis_size("sp"), lax.axis_size("tp")
+    pairs, outer = PAIR, sp_count // PAIR
+    me, my_tp = lax.axis_index("sp"), lax.axis_index("tp")
+    is_odd = (me % pairs) == 1
+    my_outer = me // pairs
+    joined = jnp.concatenate(
+        (pooling_input_weight, query_weight, key_weight, value_weight, gate_weight), axis=1
+    )
+
+    def swap(value):
+        return lax.ppermute(value, "sp", [(d, d ^ 1) for d in range(sp_count)])
+
+    def outer_shift(value, step):
+        return lax.ppermute(
+            value, "sp", [(d, (d + step * pairs) % sp_count) for d in range(sp_count)]
+        )
+
+    def tp_shift(value, step):
+        return lax.ppermute(value, "tp", [(d, (d + step) % tp_count) for d in range(tp_count)])
+
+    feature_width = inputs.shape[1]
+    gathered = jnp.zeros((tok_rows, feature_width * tp_count), inputs.dtype)
+    for step in range(tp_count):
+        piece = tp_shift(inputs, step) if step else inputs
+        gathered = lax.dynamic_update_slice_in_dim(
+            gathered, piece, ((my_tp - step) % tp_count) * feature_width, 1
+        )
+    mate_weights = swap(joined)
+    out_weights = jnp.concatenate([pooling_output_weight, delta_output_weight], axis=0)
+    out_columns = out_weights.shape[1]
+    held_weights = {0: out_weights}
+    if outer > 1:
+        held_weights[1] = outer_shift(out_weights, 1)
+    if outer > 2:
+        held_weights[outer - 1] = outer_shift(out_weights, outer - 1)
     floats = gathered.astype(jnp.float32)
     normed = (
         floats
@@ -248,40 +282,59 @@
     write_logits = rate_rows[:, head_count:]
     weights = (pooling_input_weight, query_weight, key_weight, value_weight, gate_weight)
     widths = [member.shape[1] for member in weights]
-    joined = jnp.concatenate(weights, axis=1)
-    sp_count = lax.axis_size("sp")
-    pairs, outer = PAIR, sp_count // PAIR
-    me = lax.axis_index("sp")
-    mate_weights = lax.ppermute(joined, "sp", [(d, d ^ 1) for d in range(sp_count)])
-    is_odd = (me % pairs) == 1
     depth = joined.shape[0]
-    my_outer = me // pairs
 
     def feature_block(which):
         return lax.dynamic_slice_in_dim(normed, which * (pairs * depth), pairs * depth, 1)
 
-    def outer_shift(value, step):
-        return lax.ppermute(
-            value, "sp", [(d, (d + step * pairs) % sp_count) for d in range(sp_count)]
-        )
-
-    arrived = [feature_block(my_outer)]
-    for step in range(1, outer):
-        arrived.append(outer_shift(feature_block((my_outer + step) % outer), step))
-    returned = []
-    for step in list(range(1, outer)) + [0]:
-        block = arrived[step]
+    half = outer // 2
+    arrived = {0: feature_block(my_outer)}
+    for step in [half] + [step for step in range(1, outer) if step != half]:
+        arrived[step] = outer_shift(feature_block((my_outer + step) % outer), step)
+
+    def partial_for(distance):
+        block = arrived[(outer - distance) % outer]
         mine = jnp.where(is_odd, block[:, depth:], block[:, :depth])
         other = jnp.where(is_odd, block[:, :depth], block[:, depth:])
-        partial_rows = jnp.dot(mine, joined, preferred_element_type=jnp.float32) + jnp.dot(
+        return jnp.dot(mine, joined, preferred_element_type=jnp.float32) + jnp.dot(
             other, mate_weights, preferred_element_type=jnp.float32
         )
-        if step:
-            returned.append(outer_shift(partial_rows.astype(jnp.bfloat16), outer - step))
+
+    far = partial_for(half).astype(jnp.bfloat16)
+    cut = far.shape[1] // 2
+    plus, minus = far[:, :cut], far[:, cut:]
+    for distance in range(half - 1, -1, -1):
+        got_plus = outer_shift(plus, 1).astype(jnp.float32)
+        got_minus = outer_shift(minus, outer - 1).astype(jnp.float32)
+        if distance == half - 1:
+            got_plus = jnp.pad(got_plus, ((0, 0), (0, far.shape[1] - cut)))
+            got_minus = jnp.pad(got_minus, ((0, 0), (cut, 0)))
+        if distance:
+            plus = (partial_for(distance) + got_plus).astype(jnp.bfloat16)
+            minus = (partial_for(outer - distance) + got_minus).astype(jnp.bfloat16)
         else:
-            summed_rows = partial_rows
-    for piece in returned:
-        summed_rows = summed_rows + piece.astype(jnp.float32)
+            summed_rows = partial_for(0) + got_plus + got_minus
+    half_rows = out_weights.shape[0] // 2
+    ahead, behind, summed_rows = lax.optimization_barrier(
+        (held_weights[1], held_weights[outer - 1], summed_rows)
+    )
+    for distance in range(2, half + 1):
+        if distance < half or outer % 2:
+            ahead, behind = outer_shift(ahead, 1), outer_shift(behind, outer - 1)
+            held_weights[distance], held_weights[outer - distance] = ahead, behind
+        else:
+            held_weights[distance] = jnp.concatenate(
+                [
+                    outer_shift(ahead[:half_rows], 1),
+                    outer_shift(behind[half_rows:], outer - 1),
+                ],
+                axis=0,
+            )
+    row_weights = jnp.zeros((out_weights.shape[0], outer * out_columns), out_weights.dtype)
+    for step in range(outer):
+        row_weights = lax.dynamic_update_slice_in_dim(
+            row_weights, held_weights[step], ((my_outer - step) % outer) * out_columns, 1
+        )
     split_points = [sum(widths[: split_index + 1]) for split_index in range(len(widths) - 1)]
     projected = jnp.split(summed_rows, split_points, axis=1)
     pool_rows, query_row_block, key_matrix_rows, value_row_block, gate_rows = (
@@ -339,24 +392,22 @@
     unused_state, outputs = run_blocks(state_in, terms)
     delta_out = delta_finish(outputs, gate_rows, head_norm_gain)
     both_out = jnp.concatenate([pool_out, delta_out], axis=1)
-    out_weights = jnp.concatenate([pooling_output_weight, delta_output_weight], axis=0)
-    full_weights = lax.all_gather(out_weights, "sp", axis=1, tiled=True)
-    tp_count = lax.axis_size("tp")
-    my_tp = lax.axis_index("tp")
-    width = full_weights.shape[1] // tp_count
+    mate_out = jnp.concatenate([swap(pool_out), swap(delta_out)], axis=1)
+    two_out = jnp.concatenate([both_out, mate_out], axis=0)
+    width = row_weights.shape[1] // tp_count
     sent = []
     for step in list(range(1, tp_count)) + [0]:
         columns = lax.dynamic_slice_in_dim(
-            full_weights, ((my_tp + step) % tp_count) * width, width, 1
-        )
-        part = jnp.dot(both_out, columns, preferred_element_type=jnp.float32).astype(jnp.bfloat16)
-        if step:
-            part = lax.ppermute(
-                part, "tp", [(d, (d + step) % tp_count) for d in range(tp_count)]
-            )
-        sent.append(part)
-    summed = sum(part.astype(jnp.float32) for part in sent)
-    return summed.astype(jnp.bfloat16)
+            row_weights, ((my_tp + step) % tp_count) * width, width, 1
+        )
+        part = jnp.dot(two_out, columns, preferred_element_type=jnp.float32).astype(jnp.bfloat16)
+        sent.append(tp_shift(part, step) if step else part)
+    summed = sum(part.astype(jnp.float32) for part in sent).astype(jnp.bfloat16)
+    kept = summed[:tok_rows].reshape(tok_rows, -1, 1, out_columns)
+    crossed = swap(summed[tok_rows:]).reshape(tok_rows, -1, 1, out_columns)
+    even = jnp.where(is_odd, crossed, kept)
+    odd = jnp.where(is_odd, kept, crossed)
+    return jnp.concatenate([even, odd], axis=2).reshape(tok_rows, -1)
 
 
 def solution(mesh):

time: 427 us -> 313 us (0.73)
  starting transfers between devices: 133 us -> 52.9 us
  local copies, waits for them, and re-layouts: 15.2 us -> 42.9 us
  waiting for transfers between devices: 169 us -> 142 us
  matrix products: 69.3 us -> 46.4 us
  between operations: 14.7 us -> 1.44 us
    ppermute x6 -> x11, starting transfers between devices: 89.5 us -> 27.8 us  [outer_shift(): lax.ppermute(value, 'sp', [(d, (d + step * pairs) % sp_count) for d in ra...]
    ppermute x4 -> x10, waiting for transfers between devices: 52.4 us -> 25.8 us  [the longest x6 16.8 us: tp_shift(): lax.ppermute(value, 'tp', [(d, (d + step) % tp_count) for d in range(tp_c...]
    ppermute x1, starting transfers between devices: 22.5 us -> 1.19 us  [per_device(): lax.ppermute(packed, 'sp', [(d, d ^ 1) for d in range(sp_count)])]
    all_gather x2 -> x0, waiting for transfers between devices: 13.9 us -> none  [the longest x1 13.9 us: per_device(): gathered = lax.all_gather(inputs, 'tp', axis=1, tiled=True)]
    ppermute x4, waiting for transfers between devices: 3.5 us -> 17.3 us  [shifted(): lax.ppermute(value, axis, [(source, source + steps) for source in range(l...]
    dynamic_update_slice x0 -> x7, local copies, waits for them, and re-layouts: none -> 13.6 us  [the longest x3 6.96 us: per_device(): lax.dynamic_update_slice_in_dim(row_weights, held_weights[step], (my_oute...]
    ppermute x4 -> x10, starting transfers between devices: 4.91 us -> 11.8 us  [the longest x6 7.31 us: tp_shift(): lax.ppermute(value, 'tp', [(d, (d + step) % tp_count) for d in range(tp_c...]
    dot_general x4, matrix products: 7.67 us -> 0.98 us  [advance(): jnp.einsum('hcd,hde->hce', query_decayed, state_now, precision=highest)]
  transfers between devices with their start and end apart: 17 -> 26, of which waited for: 10 -> 13; matrix products, arithmetic and copies ran while one was open for 24% -> 34% of each run, Pallas kernels for 0% -> 0%
where the time goes in v2:
time: 313 us; the launch traced here: 312 us
  waiting for transfers between devices  142 us (45%)
  starting transfers between devices  52.9 us (17%)
  matrix products  46.4 us (15%)
  local copies, waits for them, and re-layouts  42.9 us (14%)
  other arithmetic  26 us (8%)
    ppermute x11, waiting for transfers between devices, outer_shift(): lax.ppermute(value, 'sp', [(d, (d + step * pairs) % sp_count) for d in ra...  98.9 us
    ppermute x11, starting transfers between devices, outer_shift(): lax.ppermute(value, 'sp', [(d, (d + step * pairs) % sp_count) for d in ra...  27.8 us
    ppermute x4, waiting for transfers between devices, shifted(): lax.ppermute(value, axis, [(source, source + steps) for source in range(l...  17.3 us
    ppermute x6, waiting for transfers between devices, tp_shift(): lax.ppermute(value, 'tp', [(d, (d + step) % tp_count) for d in range(tp_c...  16.8 us
    ppermute x4, starting transfers between devices, shifted(): lax.ppermute(value, axis, [(source, source + steps) for source in range(l...  12.1 us
    dot_general x4, matrix products, partial_for(): jnp.dot(other, mate_weights, preferred_element_type=jnp.float32)  10.7 us
    ppermute x4, waiting for transfers between devices, swap(): return lax.ppermute(value, 'sp', [(d, d ^ 1) for d in range(sp_count)])  9.06 us
    dot_general x4, matrix products, per_device(): jnp.dot(two_out, columns, preferred_element_type=jnp.float32)  8.84 us
  transfers between devices with their start and end apart: 26, of which 13 were waited for; matrix products, arithmetic and copies ran while one was open for 34% of the time, Pallas kernels for 0%

profile of v2, /device:TPU:0, one launch (start us, length us, event | category | flops | bytes accessed | tf_op | source)
XLA Modules:
  0.0 311.8 jit_solution(10549661423336104664)
XLA Ops:
  0.6 2.6 collective-permute-start.3
  3.1 1.4 collective-permute-start.4
  8.0 1.6 collective-permute-start.5
  11.2 1.6 collective-permute-start
  18.2 1.6 broadcast_in_dim.50
  24.1 2.5 broadcast_in_dim.62
  26.6 2.3 constant_dynamic-update-slice_fusion.9
  29.0 2.3 collective-permute-start.1
  31.2 1.9 constant_dynamic-update-slice_fusion.12
  33.2 1.9 constant_dynamic-update-slice_fusion.11
  35.0 1.9 constant_dynamic-update-slice_fusion.10
  37.0 2.1 fusion
  39.1 2.2 fusion.2
  41.3 1.4 copy-done.1
  45.3 1.4 collective-permute-start.6
  46.7 2.2 fusion.180
  48.9 33.5 %collective-permute-done.7 = bf16[256,1024]{1,0:T(8,128)(2,1)} collective-permute-done((bf16[256,1024]{1,0:T(8,128)(2,1)}, bf16[256,1024]{1,0:T(8,128)(2,1)}, u32[]{:S(2)}, u32[]{:S(2)}) %collective-permute-start.7) | collective-permute-done | bytes 524320 | tf_op jit(solution)/shard_map/ppermute | solution.py:243
  82.4 10.0 %collective-permute-start.10 = (bf16[256,1024]{1,0:T(8,128)(2,1)S(1)}, bf16[256,1024]{1,0:T(8,128)(2,1)S(1)}, u32[]{:S(2)}, u32[]{:S(2)}) collective-permute-start(bf16[256,1024]{1,0:T(8,128)(2,1)S(1)} %get-tuple-element.18), channel_id=1, source_target_pairs={{0,8},{4,12},{8,16},{12,20},{16,24},{20,28},{24,0},{28,4},{1,9},{5... | collective-permute-start | bytes 1572872 | tf_op jit(solution)/shard_map/ppermute | solution.py:243
  92.3 2.8 fusion.135
  95.1 1.9 fusion.6
  97.1 3.8 %collective-permute-start.11 = (bf16[256,1280]{1,0:T(8,128)(2,1)S(1)}, bf16[256,1280]{1,0:T(8,128)(2,1)S(1)}, u32[]{:S(2)}, u32[]{:S(2)}) collective-permute-start(bf16[256,1280]{1,0:T(8,128)(2,1)S(1)} %get-tuple-element.26), channel_id=1, source_target_pairs={{0,24},{4,28},{8,0},{12,4},{16,8},{20,12},{24,16},{28,20},{1,25},{... | collective-permute-start | bytes 1966088 | tf_op jit(solution)/shard_map/ppermute | solution.py:243
  101.0 2.6 fusion.138
  103.5 4.5 %collective-permute-done.10 = bf16[256,1024]{1,0:T(8,128)(2,1)S(1)} collective-permute-done((bf16[256,1024]{1,0:T(8,128)(2,1)S(1)}, bf16[256,1024]{1,0:T(8,128)(2,1)S(1)}, u32[]{:S(2)}, u32[]{:S(2)}) %collective-permute-start.10) | collective-permute-done | bytes 524320 | tf_op jit(solution)/shard_map/ppermute | solution.py:243
  108.0 2.6 fusion.132
  110.6 11.4 %collective-permute-done.8 = bf16[256,1280]{1,0:T(8,128)(2,1)S(1)} collective-permute-done((bf16[256,1280]{1,0:T(8,128)(2,1)S(1)}, bf16[256,1280]{1,0:T(8,128)(2,1)S(1)}, u32[]{:S(2)}, u32[]{:S(2)}) %collective-permute-start.8) | collective-permute-done | bytes 655392 | tf_op jit(solution)/shard_map/ppermute | solution.py:243
  122.0 2.0 fusion.5
  124.0 11.9 %collective-permute-done.11 = bf16[256,1280]{1,0:T(8,128)(2,1)S(1)} collective-permute-done((bf16[256,1280]{1,0:T(8,128)(2,1)S(1)}, bf16[256,1280]{1,0:T(8,128)(2,1)S(1)}, u32[]{:S(2)}, u32[]{:S(2)}) %collective-permute-start.11) | collective-permute-done | bytes 655392 | tf_op jit(solution)/shard_map/ppermute | solution.py:243
  136.0 1.9 fusion.7
  137.9 4.1 %collective-permute-start.12 = (bf16[256,2560]{1,0:T(8,128)(2,1)}, bf16[256,2560]{1,0:T(8,128)(2,1)}, u32[]{:S(2)}, u32[]{:S(2)}) collective-permute-start(bf16[256,2560]{1,0:T(8,128)(2,1)} %fusion.7), channel_id=1, source_target_pairs={{0,24},{4,28},{8,0},{12,4},{16,8},{20,12},{24,16},{28,20},{1,25},{... | collective-permute-start | bytes 3932168 | tf_op jit(solution)/shard_map/ppermute | solution.py:243
  147.2 1.9 fusion.143
  149.1 2.3 constant_dynamic-update-slice_fusion.8
  151.4 2.8 fusion.141
  154.1 15.9 %collective-permute-done.9 = bf16[256,2560]{1,0:T(8,128)(2,1)} collective-permute-done((bf16[256,2560]{1,0:T(8,128)(2,1)}, bf16[256,2560]{1,0:T(8,128)(2,1)}, u32[]{:S(2)}, u32[]{:S(2)}) %collective-permute-start.9) | collective-permute-done | bytes 1310752 | tf_op jit(solution)/shard_map/ppermute | solution.py:243
  170.0 21.7 %collective-permute-done.12 = bf16[256,2560]{1,0:T(8,128)(2,1)} collective-permute-done((bf16[256,2560]{1,0:T(8,128)(2,1)}, bf16[256,2560]{1,0:T(8,128)(2,1)}, u32[]{:S(2)}, u32[]{:S(2)}) %collective-permute-start.12) | collective-permute-done | bytes 1310752 | tf_op jit(solution)/shard_map/ppermute | solution.py:243
  191.7 2.5 convert_add_fusion
  195.4 1.3 fusion.212
  196.7 3.1 %collective-permute-start.13 = (bf16[16,512]{1,0:T(8,128)(2,1)}, bf16[16,512]{1,0:T(8,128)(2,1)}, u32[]{:S(2)}, u32[]{:S(2)}) collective-permute-start(bf16[16,512]{1,0:T(8,128)(2,1)} %slice.363), channel_id=1, source_target_pairs={{0,4},{4,8},{8,12},{12,16},{16,20},{20,24},{24,28},{1,5},{5,9},{9,... | collective-permute-start | bytes 49160 | tf_op jit(solution)/shard_map/ppermute | solution.py:19
  204.1 1.2 multiply_multiply_fusion
  205.3 1.3 fusion.9
  214.4 1.2 collective-permute-start.14
  215.6 1.5 fusion.10
  217.0 1.2 bitcast_multiply_fusion.20
  218.2 1.9 slice.351
  220.7 1.9 slice.352
  222.6 3.2 %collective-permute-start.21 = (bf16[512,512]{1,0:T(8,128)(2,1)}, bf16[512,512]{1,0:T(8,128)(2,1)}, u32[]{:S(2)}, u32[]{:S(2)}) collective-permute-start(bf16[512,512]{1,0:T(8,128)(2,1)} %slice.352), channel_id=1, source_target_pairs={{0,24},{4,28},{8,0},{12,4},{16,8},{20,12},{24,16},{28,20},{1,25},{... | collective-permute-start | bytes 1572872 | tf_op jit(solution)/shard_map/ppermute | solution.py:243
  228.1 1.3 collective-permute-start.15
  229.7 15.8 %collective-permute-done.15 = bf16[4,128,128]{2,1,0:T(8,128)(2,1)S(1)} collective-permute-done((bf16[4,128,128]{2,1,0:T(8,128)(2,1)S(1)}, bf16[4,128,128]{2,1,0:T(8,128)(2,1)S(1)}, u32[]{:S(2)}, u32[]{:S(2)}) %collective-permute-start.15) | collective-permute-done | bytes 131104 | tf_op jit(solution)/shard_map/ppermute | solution.py:19
  245.7 4.4 %collective-permute-start.16 = (bf16[4,128,128]{2,1,0:T(8,128)(2,1)S(1)}, bf16[4,128,128]{2,1,0:T(8,128)(2,1)S(1)}, u32[]{:S(2)}, u32[]{:S(2)}) collective-permute-start(bf16[4,128,128]{2,1,0:T(8,128)(2,1)S(1)} %fusion.12), channel_id=1, source_target_pairs={{0,8},{4,12},{8,16},{12,20},{16,24},{20,28},{1,9},{5,13},{9,17},{1... | collective-permute-start | bytes 393224 | tf_op jit(solution)/shard_map/ppermute | solution.py:19
  250.3 2.1 fusion.45
  252.5 1.2 copy.186
  254.0 3.3 %collective-permute-start.17 = (bf16[4,128,128]{2,1,0:T(8,128)(2,1)S(1)}, bf16[4,128,128]{2,1,0:T(8,128)(2,1)S(1)}, u32[]{:S(2)}, u32[]{:S(2)}) collective-permute-start(bf16[4,128,128]{2,1,0:T(8,128)(2,1)S(1)} %fusion.13), channel_id=1, source_target_pairs={{0,8},{4,12},{8,16},{12,20},{16,24},{20,28},{1,9},{5,13},{9,17},{1... | collective-permute-start | bytes 393224 | tf_op jit(solution)/shard_map/ppermute | solution.py:19
  258.3 1.5 collective-permute-done.17
  267.3 2.3 maximum_dynamic-update-slice_fusion
  269.6 2.3 constant_dynamic-update-slice_fusion.7
  272.7 2.0 convolution_convert_fusion.3
  274.8 2.1 convolution_convert_fusion.2
  276.9 1.3 collective-permute-start.23
  278.2 2.7 convolution_convert_fusion.1
  281.0 1.4 collective-permute-start.24
  282.4 3.9 %collective-permute-done.22 = bf16[512,512]{1,0:T(8,128)(2,1)S(1)} collective-permute-done((bf16[512,512]{1,0:T(8,128)(2,1)S(1)}, bf16[512,512]{1,0:T(8,128)(2,1)S(1)}, u32[]{:S(2)}, u32[]{:S(2)}) %collective-permute-start.22) | collective-permute-done | bytes 524320 | tf_op jit(solution)/shard_map/ppermute | solution.py:248
  286.3 5.5 %collective-permute-done.23 = bf16[512,512]{1,0:T(8,128)(2,1)S(1)} collective-permute-done((bf16[512,512]{1,0:T(8,128)(2,1)S(1)}, bf16[512,512]{1,0:T(8,128)(2,1)S(1)}, u32[]{:S(2)}, u32[]{:S(2)}) %collective-permute-start.23) | collective-permute-done | bytes 524320 | tf_op jit(solution)/shard_map/ppermute | solution.py:248
  291.8 7.4 %collective-permute-done.24 = bf16[512,512]{1,0:T(8,128)(2,1)S(1)} collective-permute-done((bf16[512,512]{1,0:T(8,128)(2,1)}, bf16[512,512]{1,0:T(8,128)(2,1)S(1)}, u32[]{:S(2)}, u32[]{:S(2)}) %collective-permute-start.24) | collective-permute-done | bytes 524320 | tf_op jit(solution)/shard_map/ppermute | solution.py:248
  299.2 2.0 add_convert_fusion
  302.2 8.2 %collective-permute-done.25 = bf16[256,512]{1,0:T(8,128)(2,1)S(1)} collective-permute-done((bf16[256,512]{1,0:T(8,128)(2,1)S(1)}, bf16[256,512]{1,0:T(8,128)(2,1)S(1)}, u32[]{:S(2)}, u32[]{:S(2)}) %collective-permute-start.25) | collective-permute-done | bytes 262176 | tf_op jit(solution)/shard_map/ppermute | solution.py:240
  (248 shorter events, 50.9 us)
Async XLA Ops:
  0.0 250.1 %copy-start = (bf16[4,128,128]{2,1,0:T(8,128)(2,1)S(1)}, bf16[4,128,128]{2,1,0:T(8,128)(2,1)}, u32[]{:S(2)}) copy-start(bf16[4,128,128]{2,1,0:T(8,128)(2,1)} %param.28) | copy-start | bytes 393220
  0.0 7.8 %copy-start.7 = (bf16[512,512]{1,0:T(8,128)(2,1)S(1)}, bf16[512,512]{1,0:T(8,128)(2,1)}, u32[]{:S(2)}) copy-start(bf16[512,512]{1,0:T(8,128)(2,1)} %param.24) | copy-start | bytes 1572868
  0.0 7.9 %copy-start.8 = (bf16[512,512]{1,0:T(8,128)(2,1)S(1)}, bf16[512,512]{1,0:T(8,128)(2,1)}, u32[]{:S(2)}) copy-start(bf16[512,512]{1,0:T(8,128)(2,1)} %param.25) | copy-start | bytes 1572868
  0.0 9.5 %copy-start.9 = (bf16[512,512]{1,0:T(8,128)(2,1)S(1)}, bf16[512,512]{1,0:T(8,128)(2,1)}, u32[]{:S(2)}) copy-start(bf16[512,512]{1,0:T(8,128)(2,1)} %param.36) | copy-start | bytes 1572868
  0.0 28.9 %collective-permute-start.2 = (bf16[256,1024]{1,0:T(8,128)(2,1)}, bf16[256,1024]{1,0:T(8,128)(2,1)}, u32[]{:S(2)}, u32[]{:S(2)}) collective-permute-start(bf16[256,1024]{1,0:T(8,128)(2,1)} %param.19), channel_id=1, source_target_pairs={{0,1},{1,2},{2,3},{3,0},{4,5},{5,6},{6,7},{7,4},{8,9},{9,10},{10,1... | collective-permute-start | bytes 1572872 | tf_op jit(solution)/shard_map/ppermute | solution.py:248
  0.6 32.6 %collective-permute-start.3 = (bf16[256,1024]{1,0:T(8,128)(2,1)}, bf16[256,1024]{1,0:T(8,128)(2,1)}, u32[]{:S(2)}, u32[]{:S(2)}) collective-permute-start(bf16[256,1024]{1,0:T(8,128)(2,1)} %param.19), channel_id=1, source_target_pairs={{0,2},{1,3},{2,0},{3,1},{4,6},{5,7},{6,4},{7,5},{8,10},{9,11},{10,... | collective-permute-start | bytes 1572872 | tf_op jit(solution)/shard_map/ppermute | solution.py:248
  3.1 31.9 %collective-permute-start.4 = (bf16[256,1024]{1,0:T(8,128)(2,1)}, bf16[256,1024]{1,0:T(8,128)(2,1)}, u32[]{:S(2)}, u32[]{:S(2)}) collective-permute-start(bf16[256,1024]{1,0:T(8,128)(2,1)} %param.19), channel_id=1, source_target_pairs={{0,3},{1,0},{2,1},{3,2},{4,7},{5,4},{6,5},{7,6},{8,11},{9,8},{10,9... | collective-permute-start | bytes 1572872 | tf_op jit(solution)/shard_map/ppermute | solution.py:248
  5.6 4.8 %copy-start.10 = (bf16[512,512]{1,0:T(8,128)(2,1)S(1)}, bf16[512,512]{1,0:T(8,128)(2,1)}, u32[]{:S(2)}) copy-start(bf16[512,512]{1,0:T(8,128)(2,1)} %param.37) | copy-start | bytes 1572868
  6.7 10.9 %copy-start.54 = (f32[4]{0:T(128)S(1)}, f32[4]{0:T(128)}, u32[]{:S(2)}) copy-start(f32[4]{0:T(128)} %param.30) | copy-start | bytes 52
  6.7 10.9 %copy-start.48 = (f32[128]{0:T(128)S(1)}, f32[128]{0:T(128)}, u32[]{:S(2)}) copy-start(f32[128]{0:T(128)} %param.35) | copy-start | bytes 1540
  7.9 11.9 %copy-start.11 = (bf16[256,1024]{1,0:T(8,128)(2,1)S(1)}, bf16[256,1024]{1,0:T(8,128)(2,1)}, u32[]{:S(2)}) copy-start(bf16[256,1024]{1,0:T(8,128)(2,1)} %param.19) | copy-start | bytes 1572868
  8.0 84.4 %collective-permute-start.5 = (bf16[512,2560]{1,0:T(8,128)(2,1)S(1)}, bf16[512,2560]{1,0:T(8,128)(2,1)}, u32[]{:S(2)}, u32[]{:S(2)}) collective-permute-start(bf16[512,2560]{1,0:T(8,128)(2,1)S(1)} %constant_dynamic-update-slice_fusion.2), channel_id=1, source_target_pairs={{0,4},{4,0},{8,12},{12,8},{16,20},{20,16},{24,28},{28,24},{1,5},{5... | collective-permute-start | bytes 7864328 | tf_op jit(solution)/shard_map/ppermute | solution.py:240
  11.2 137.8 %collective-permute-start = (bf16[1024,512]{1,0:T(8,128)(2,1)}, bf16[1024,512]{1,0:T(8,128)(2,1)}, u32[]{:S(2)}, u32[]{:S(2)}) collective-permute-start(bf16[1024,512]{1,0:T(8,128)(2,1)} %constant_dynamic-update-slice_fusion), channel_id=1, source_target_pairs={{0,8},{4,12},{8,16},{12,20},{16,24},{20,28},{24,0},{28,4},{1,9},{5... | collective-permute-start | bytes 3145736 | tf_op jit(solution)/shard_map/ppermute | solution.py:243
  24.1 4.8 %copy-start.23 = (bf16[4096]{0:T(1024)(128)(2,1)S(1)}, bf16[4096]{0:T(1024)(128)(2,1)}, u32[]{:S(2)}) copy-start(bf16[4096]{0:T(1024)(128)(2,1)} %param.20) | copy-start | bytes 24580
  29.0 165.3 %collective-permute-start.1 = (bf16[1024,512]{1,0:T(8,128)(2,1)}, bf16[1024,512]{1,0:T(8,128)(2,1)}, u32[]{:S(2)}, u32[]{:S(2)}) collective-permute-start(bf16[1024,512]{1,0:T(8,128)(2,1)} %constant_dynamic-update-slice_fusion), channel_id=1, source_target_pairs={{0,24},{4,28},{8,0},{12,4},{16,8},{20,12},{24,16},{28,20},{1,25},{... | collective-permute-start | bytes 3145736 | tf_op jit(solution)/shard_map/ppermute | solution.py:243
  43.8 38.6 %collective-permute-start.7 = (bf16[256,1024]{1,0:T(8,128)(2,1)}, bf16[256,1024]{1,0:T(8,128)(2,1)}, u32[]{:S(2)}, u32[]{:S(2)}) collective-permute-start(bf16[256,1024]{1,0:T(8,128)(2,1)} %get-tuple-element.19), channel_id=1, source_target_pairs={{0,16},{4,20},{8,24},{12,28},{16,0},{20,4},{24,8},{28,12},{1,17},{... | collective-permute-start | bytes 1572872 | tf_op jit(solution)/shard_map/ppermute | solution.py:243
  45.3 51.8 %collective-permute-start.6 = (bf16[256,1024]{1,0:T(8,128)(2,1)}, bf16[256,1024]{1,0:T(8,128)(2,1)S(1)}, u32[]{:S(2)}, u32[]{:S(2)}) collective-permute-start(bf16[256,1024]{1,0:T(8,128)(2,1)} %get-tuple-element.17), channel_id=1, source_target_pairs={{0,24},{4,28},{8,0},{12,4},{16,8},{20,12},{24,16},{28,20},{1,25},{... | collective-permute-start | bytes 1572872 | tf_op jit(solution)/shard_map/ppermute | solution.py:243
  82.4 25.6 %collective-permute-start.10 = (bf16[256,1024]{1,0:T(8,128)(2,1)S(1)}, bf16[256,1024]{1,0:T(8,128)(2,1)S(1)}, u32[]{:S(2)}, u32[]{:S(2)}) collective-permute-start(bf16[256,1024]{1,0:T(8,128)(2,1)S(1)} %get-tuple-element.18), channel_id=1, source_target_pairs={{0,8},{4,12},{8,16},{12,20},{16,24},{20,28},{24,0},{28,4},{1,9},{5... | collective-permute-start | bytes 1572872 | tf_op jit(solution)/shard_map/ppermute | solution.py:243
  97.1 24.9 %collective-permute-start.8 = (bf16[256,1280]{1,0:T(8,128)(2,1)S(1)}, bf16[256,1280]{1,0:T(8,128)(2,1)S(1)}, u32[]{:S(2)}, u32[]{:S(2)}) collective-permute-start(bf16[256,1280]{1,0:T(8,128)(2,1)S(1)} %get-tuple-element.25), channel_id=1, source_target_pairs={{0,8},{4,12},{8,16},{12,20},{16,24},{20,28},{24,0},{28,4},{1,9},{5... | collective-permute-start | bytes 1966088 | tf_op jit(solution)/shard_map/ppermute | solution.py:243
  97.1 38.8 %collective-permute-start.11 = (bf16[256,1280]{1,0:T(8,128)(2,1)S(1)}, bf16[256,1280]{1,0:T(8,128)(2,1)S(1)}, u32[]{:S(2)}, u32[]{:S(2)}) collective-permute-start(bf16[256,1280]{1,0:T(8,128)(2,1)S(1)} %get-tuple-element.26), channel_id=1, source_target_pairs={{0,24},{4,28},{8,0},{12,4},{16,8},{20,12},{24,16},{28,20},{1,25},{... | collective-permute-start | bytes 1966088 | tf_op jit(solution)/shard_map/ppermute | solution.py:243
  124.0 18.0 %copy-start.28 = (f32[256,4]{0,1:T(4,128)S(1)}, f32[256,4]{0,1:T(4,128)}, u32[]{:S(2)}) copy-start(f32[256,4]{0,1:T(4,128)} %param.34) | copy-start | bytes 12292
  124.0 18.0 %copy-start.29 = (f32[256,4]{0,1:T(4,128)S(1)}, f32[256,4]{0,1:T(4,128)}, u32[]{:S(2)}) copy-start(f32[256,4]{0,1:T(4,128)} %param.33) | copy-start | bytes 12292
  124.0 18.0 %copy-start.49 = (f32[4]{0:T(128)S(1)}, f32[4]{0:T(128)}, u32[]{:S(2)}) copy-start(f32[4]{0:T(128)} %param.32) | copy-start | bytes 52
  124.0 18.0 %copy-start.50 = (f32[4]{0:T(128)S(1)}, f32[4]{0:T(128)}, u32[]{:S(2)}) copy-start(f32[4]{0:T(128)} %param.31) | copy-start | bytes 52
  124.0 46.1 %collective-permute-start.9 = (bf16[256,2560]{1,0:T(8,128)(2,1)}, bf16[256,2560]{1,0:T(8,128)(2,1)}, u32[]{:S(2)}, u32[]{:S(2)}) collective-permute-start(bf16[256,2560]{1,0:T(8,128)(2,1)} %fusion.5), channel_id=1, source_target_pairs={{0,8},{4,12},{8,16},{12,20},{16,24},{20,28},{24,0},{28,4},{1,9},{5... | collective-permute-start | bytes 3932168 | tf_op jit(solution)/shard_map/ppermute | solution.py:243
  137.9 53.9 %collective-permute-start.12 = (bf16[256,2560]{1,0:T(8,128)(2,1)}, bf16[256,2560]{1,0:T(8,128)(2,1)}, u32[]{:S(2)}, u32[]{:S(2)}) collective-permute-start(bf16[256,2560]{1,0:T(8,128)(2,1)} %fusion.7), channel_id=1, source_target_pairs={{0,24},{4,28},{8,0},{12,4},{16,8},{20,12},{24,16},{28,20},{1,25},{... | collective-permute-start | bytes 3932168 | tf_op jit(solution)/shard_map/ppermute | solution.py:243
  196.7 4.6 %copy-start.5 = (f32[256,512]{1,0:T(8,128)S(1)}, f32[256,512]{1,0:T(8,128)}, u32[]{:S(2)}) copy-start(f32[256,512]{1,0:T(8,128)} %get-tuple-element.21) | copy-start | bytes 1572868
  196.7 29.1 %collective-permute-start.13 = (bf16[16,512]{1,0:T(8,128)(2,1)}, bf16[16,512]{1,0:T(8,128)(2,1)}, u32[]{:S(2)}, u32[]{:S(2)}) collective-permute-start(bf16[16,512]{1,0:T(8,128)(2,1)} %slice.363), channel_id=1, source_target_pairs={{0,4},{4,8},{8,12},{12,16},{16,20},{20,24},{24,28},{1,5},{5,9},{9,... | collective-permute-start | bytes 49160 | tf_op jit(solution)/shard_map/ppermute | solution.py:19
  213.8 3.2 %copy-start.19 = (f32[4,4,64]{2,1,0:T(4,128)S(1)}, f32[4,4,64]{2,1,0:T(4,128)}, u32[]{:S(2)}) copy-start(f32[4,4,64]{2,1,0:T(4,128)} %copy.171) | copy-start | bytes 12292
  214.4 13.4 %collective-permute-start.14 = (bf16[2,4,128,128]{3,2,1,0:T(8,128)(2,1)S(1)}, bf16[2,4,128,128]{3,2,1,0:T(8,128)(2,1)S(1)}, u32[]{:S(2)}, u32[]{:S(2)}) collective-permute-start(bf16[2,4,128,128]{3,2,1,0:T(8,128)(2,1)S(1)} %fusion.106), channel_id=1, source_target_pairs={{0,4},{4,0},{8,12},{12,8},{16,20},{20,16},{24,28},{28,24},{1,5},{5... | collective-permute-start | bytes 786440 | tf_op jit(solution)/shard_map/ppermute | solution.py:377
  220.1 47.1 %collective-permute-start.20 = (bf16[512,512]{1,0:T(8,128)(2,1)}, bf16[512,512]{1,0:T(8,128)(2,1)}, u32[]{:S(2)}, u32[]{:S(2)}) collective-permute-start(bf16[512,512]{1,0:T(8,128)(2,1)} %slice.351), channel_id=1, source_target_pairs={{0,8},{4,12},{8,16},{12,20},{16,24},{20,28},{24,0},{28,4},{1,9},{5... | collective-permute-start | bytes 1572872 | tf_op jit(solution)/shard_map/ppermute | solution.py:243
  222.6 44.7 %collective-permute-start.21 = (bf16[512,512]{1,0:T(8,128)(2,1)}, bf16[512,512]{1,0:T(8,128)(2,1)}, u32[]{:S(2)}, u32[]{:S(2)}) collective-permute-start(bf16[512,512]{1,0:T(8,128)(2,1)} %slice.352), channel_id=1, source_target_pairs={{0,24},{4,28},{8,0},{12,4},{16,8},{20,12},{24,16},{28,20},{1,25},{... | collective-permute-start | bytes 1572872 | tf_op jit(solution)/shard_map/ppermute | solution.py:243
  227.6 22.6 %copy-start.21 = (f32[256,4]{0,1:T(4,128)S(1)}, f32[256,4]{0,1:T(4,128)}, u32[]{:S(2)}) copy-start(f32[256,4]{0,1:T(4,128)} %minimum_convert_fusion) | copy-start | bytes 12292
  227.6 22.6 %copy-start.32 = (f32[4]{0:T(128)S(1)}, f32[4]{0:T(128)}, u32[]{:S(2)}) copy-start(f32[4]{0:T(128)} %get-tuple-element.67) | copy-start | bytes 52
  227.6 22.6 %copy-start.33 = (f32[4]{0:T(128)S(1)}, f32[4]{0:T(128)}, u32[]{:S(2)}) copy-start(f32[4]{0:T(128)} %get-tuple-element.68) | copy-start | bytes 52
  227.6 22.6 %copy-start.34 = (f32[4]{0:T(128)S(1)}, f32[4]{0:T(128)}, u32[]{:S(2)}) copy-start(f32[4]{0:T(128)} %get-tuple-element.69) | copy-start | bytes 52
  227.6 22.6 %copy-start.35 = (f32[4]{0:T(128)S(1)}, f32[4]{0:T(128)}, u32[]{:S(2)}) copy-start(f32[4]{0:T(128)} %get-tuple-element.70) | copy-start | bytes 52
  227.6 22.6 %copy-start.36 = (f32[4]{0:T(128)S(1)}, f32[4]{0:T(128)}, u32[]{:S(2)}) copy-start(f32[4]{0:T(128)} %get-tuple-element.71) | copy-start | bytes 52
  227.6 22.6 %copy-start.37 = (f32[4]{0:T(128)S(1)}, f32[4]{0:T(128)}, u32[]{:S(2)}) copy-start(f32[4]{0:T(128)} %get-tuple-element.72) | copy-start | bytes 52
  227.6 22.6 %copy-start.38 = (f32[4]{0:T(128)S(1)}, f32[4]{0:T(128)}, u32[]{:S(2)}) copy-start(f32[4]{0:T(128)} %get-tuple-element.73) | copy-start | bytes 52
  227.6 22.6 %copy-start.39 = (f32[4]{0:T(128)S(1)}, f32[4]{0:T(128)}, u32[]{:S(2)}) copy-start(f32[4]{0:T(128)} %get-tuple-element.74) | copy-start | bytes 52
  227.6 22.6 %copy-start.40 = (f32[4]{0:T(128)S(1)}, f32[4]{0:T(128)}, u32[]{:S(2)}) copy-start(f32[4]{0:T(128)} %get-tuple-element.75) | copy-start | bytes 52
  227.7 22.6 %copy-start.41 = (f32[4]{0:T(128)S(1)}, f32[4]{0:T(128)}, u32[]{:S(2)}) copy-start(f32[4]{0:T(128)} %get-tuple-element.76) | copy-start | bytes 52
  227.7 22.6 %copy-start.42 = (f32[4]{0:T(128)S(1)}, f32[4]{0:T(128)}, u32[]{:S(2)}) copy-start(f32[4]{0:T(128)} %get-tuple-element.77) | copy-start | bytes 52
  227.7 22.6 %copy-start.43 = (f32[4]{0:T(128)S(1)}, f32[4]{0:T(128)}, u32[]{:S(2)}) copy-start(f32[4]{0:T(128)} %get-tuple-element.78) | copy-start | bytes 52
  227.7 22.6 %copy-start.44 = (f32[4]{0:T(128)S(1)}, f32[4]{0:T(128)}, u32[]{:S(2)}) copy-start(f32[4]{0:T(128)} %get-tuple-element.79) | copy-start | bytes 52
  227.7 22.6 %copy-start.45 = (f32[4]{0:T(128)S(1)}, f32[4]{0:T(128)}, u32[]{:S(2)}) copy-start(f32[4]{0:T(128)} %get-tuple-element.80) | copy-start | bytes 52
  227.7 22.6 %copy-start.46 = (f32[4]{0:T(128)S(1)}, f32[4]{0:T(128)}, u32[]{:S(2)}) copy-start(f32[4]{0:T(128)} %get-tuple-element.81) | copy-start | bytes 52
  227.7 22.6 %copy-start.47 = (f32[4]{0:T(128)S(1)}, f32[4]{0:T(128)}, u32[]{:S(2)}) copy-start(f32[4]{0:T(128)} %get-tuple-element.82) | copy-start | bytes 52
  228.1 17.4 %collective-permute-start.15 = (bf16[4,128,128]{2,1,0:T(8,128)(2,1)S(1)}, bf16[4,128,128]{2,1,0:T(8,128)(2,1)S(1)}, u32[]{:S(2)}, u32[]{:S(2)}) collective-permute-start(bf16[4,128,128]{2,1,0:T(8,128)(2,1)S(1)} %get-tuple-element.63), channel_id=1, source_target_pairs={{0,8},{4,12},{8,16},{12,20},{16,24},{20,28},{1,9},{5,13},{9,17},{1... | collective-permute-start | bytes 393224 | tf_op jit(solution)/shard_map/ppermute | solution.py:19
  245.7 8.0 %collective-permute-start.16 = (bf16[4,128,128]{2,1,0:T(8,128)(2,1)S(1)}, bf16[4,128,128]{2,1,0:T(8,128)(2,1)S(1)}, u32[]{:S(2)}, u32[]{:S(2)}) collective-permute-start(bf16[4,128,128]{2,1,0:T(8,128)(2,1)S(1)} %fusion.12), channel_id=1, source_target_pairs={{0,8},{4,12},{8,16},{12,20},{16,24},{20,28},{1,9},{5,13},{9,17},{1... | collective-permute-start | bytes 393224 | tf_op jit(solution)/shard_map/ppermute | solution.py:19
  250.3 6.9 %copy-start.30 = (f32[512]{0:T(512)S(1)}, f32[512]{0:T(512)}, u32[]{:S(2)}) copy-start(f32[512]{0:T(512)} %param.29) | copy-start | bytes 6148
  253.7 6.9 %copy-start.6 = (f32[4,4,64,64]{3,2,1,0:T(8,128)S(1)}, f32[4,4,64,64]{3,2,1,0:T(8,128)}, u32[]{:S(2)}) copy-start(f32[4,4,64,64]{3,2,1,0:T(8,128)} %fusion.10) | copy-start | bytes 786436
  254.0 5.8 %collective-permute-start.17 = (bf16[4,128,128]{2,1,0:T(8,128)(2,1)S(1)}, bf16[4,128,128]{2,1,0:T(8,128)(2,1)S(1)}, u32[]{:S(2)}, u32[]{:S(2)}) collective-permute-start(bf16[4,128,128]{2,1,0:T(8,128)(2,1)S(1)} %fusion.13), channel_id=1, source_target_pairs={{0,8},{4,12},{8,16},{12,20},{16,24},{20,28},{1,9},{5,13},{9,17},{1... | collective-permute-start | bytes 393224 | tf_op jit(solution)/shard_map/ppermute | solution.py:19
  257.3 14.6 %collective-permute-start.18 = (bf16[256,512]{1,0:T(8,128)(2,1)S(1)}, bf16[256,512]{1,0:T(8,128)(2,1)S(1)}, u32[]{:S(2)}, u32[]{:S(2)}) collective-permute-start(bf16[256,512]{1,0:T(8,128)(2,1)S(1)} %multiply_convert_fusion), channel_id=1, source_target_pairs={{0,4},{4,0},{8,12},{12,8},{16,20},{20,16},{24,28},{28,24},{1,5},{5... | collective-permute-start | bytes 786440 | tf_op jit(solution)/shard_map/ppermute | solution.py:240
  260.0 2.6 copy-start.3
  266.3 6.4 %collective-permute-start.19 = (bf16[256,512]{1,0:T(8,128)(2,1)S(1)}, bf16[256,512]{1,0:T(8,128)(2,1)S(1)}, u32[]{:S(2)}, u32[]{:S(2)}) collective-permute-start(bf16[256,512]{1,0:T(8,128)(2,1)S(1)} %fusion.100), channel_id=1, source_target_pairs={{0,4},{4,0},{8,12},{12,8},{16,20},{20,16},{24,28},{28,24},{1,5},{5... | collective-permute-start | bytes 786440 | tf_op jit(solution)/shard_map/ppermute | solution.py:240
  271.9 2.9 copy-start.51
  272.7 5.5 %copy-start.53 = (bf16[256,512]{1,0:T(8,128)(2,1)}, bf16[256,512]{1,0:T(8,128)(2,1)S(1)}, u32[]{:S(2)}) copy-start(bf16[256,512]{1,0:T(8,128)(2,1)S(1)} %collective-permute-done.19) | copy-start | bytes 786436
  274.8 11.5 %collective-permute-start.22 = (bf16[512,512]{1,0:T(8,128)(2,1)S(1)}, bf16[512,512]{1,0:T(8,128)(2,1)S(1)}, u32[]{:S(2)}, u32[]{:S(2)}) collective-permute-start(bf16[512,512]{1,0:T(8,128)(2,1)S(1)} %convolution_convert_fusion.3), channel_id=1, source_target_pairs={{0,1},{1,2},{2,3},{3,0},{4,5},{5,6},{6,7},{7,4},{8,9},{9,10},{10,1... | collective-permute-start | bytes 1572872 | tf_op jit(solution)/shard_map/ppermute | solution.py:248
  274.8 3.4 %copy-start.52 = (bf16[256,512]{1,0:T(8,128)(2,1)S(1)}, bf16[256,512]{1,0:T(8,128)(2,1)}, u32[]{:S(2)}) copy-start(bf16[256,512]{1,0:T(8,128)(2,1)} %copy-done.51) | copy-start | bytes 786436
  276.9 14.9 %collective-permute-start.23 = (bf16[512,512]{1,0:T(8,128)(2,1)S(1)}, bf16[512,512]{1,0:T(8,128)(2,1)S(1)}, u32[]{:S(2)}, u32[]{:S(2)}) collective-permute-start(bf16[512,512]{1,0:T(8,128)(2,1)S(1)} %convolution_convert_fusion.2), channel_id=1, source_target_pairs={{0,2},{1,3},{2,0},{3,1},{4,6},{5,7},{6,4},{7,5},{8,10},{9,11},{10,... | collective-permute-start | bytes 1572872 | tf_op jit(solution)/shard_map/ppermute | solution.py:248
  281.0 18.2 %collective-permute-start.24 = (bf16[512,512]{1,0:T(8,128)(2,1)}, bf16[512,512]{1,0:T(8,128)(2,1)S(1)}, u32[]{:S(2)}, u32[]{:S(2)}) collective-permute-start(bf16[512,512]{1,0:T(8,128)(2,1)} %convolution_convert_fusion.1), channel_id=1, source_target_pairs={{0,3},{1,0},{2,1},{3,2},{4,7},{5,4},{6,5},{7,6},{8,11},{9,8},{10,9... | collective-permute-start | bytes 1572872 | tf_op jit(solution)/shard_map/ppermute | solution.py:248
  301.2 9.2 %collective-permute-start.25 = (bf16[256,512]{1,0:T(8,128)(2,1)S(1)}, bf16[256,512]{1,0:T(8,128)(2,1)S(1)}, u32[]{:S(2)}, u32[]{:S(2)}) collective-permute-start(bf16[256,512]{1,0:T(8,128)(2,1)S(1)} %slice.411), channel_id=1, source_target_pairs={{0,4},{4,0},{8,12},{12,8},{16,20},{20,16},{24,28},{28,24},{1,5},{5... | collective-permute-start | bytes 786440 | tf_op jit(solution)/shard_map/ppermute | solution.py:240
  (17 other events, 29.3 us)
